TPU v7x, 32 devices: a whole 2x2x4 slice. The times are simulated.
32 devices in a mesh: sp: 16 (over z, y, x), tp: 2 (over core).
Axes of the slice: x: 2, y: 2, z: 4, core: 2. Of those that a mesh axis runs over, the one named last changes fastest.
Arguments:
- head_value_rows: bfloat16 [12288, 2048], P('sp', 'tp'), may hold values from -6 to 6
- entry_map_rows: bfloat16 [12288, 1024], P('sp', 'tp'), may hold values from -6 to 6
- readout_map_rows: bfloat16 [12288, 1024], P('sp', 'tp'), may hold values from -6 to 6
- output_gate_rows: bfloat16 [12288, 2048], P('sp', 'tp'), may hold values from -6 to 6
- step_before_softplus: bfloat16 [12288, 32], P('sp', 'tp'), may hold values from -8 to 8
- sudden_log_decay: float32 [12288, 32], P('sp', 'tp'), may hold values from -1 to 0
- document_index: int32 [12288], replicated, may hold values from 0 to 3, never falling along the last dimension, each value on 1 to 6144 neighbouring positions
- head_rate_logarithm: float32 [2, 32], P(None, 'tp'), may hold values from -30 to 0
- head_step_bias: float32 [2, 32], P(None, 'tp'), may hold values from -3 to 3
- value_conv_taps: bfloat16 [5, 2048], P(None, 'tp'), may hold values from -2.5 to 2.5
- entry_conv_taps: bfloat16 [5, 1024], P(None, 'tp'), may hold values from -2.5 to 2.5
- readout_conv_taps: bfloat16 [5, 1024], P(None, 'tp'), may hold values from -2.5 to 2.5
- group_norm_gain: float32 [2048], P('tp'), may hold values from 0.1 to 1.9
- mixer_output_weight: bfloat16 [2048, 2048], P('tp'), may hold values from -0.125 to 0.125
- stream: bfloat16 [12288, 2048], P('sp', 'tp'), may hold values from -200 to 200
- mixer_norm_gain: float32 [2048], P('tp'), may hold values from 0.1 to 1.9
- channel_norm_gain: float32 [2048], P('tp'), may hold values from 0.1 to 1.9
- up_projection_weight: bfloat16 [2048, 8192], P('sp', 'tp'), may hold values from -0.125 to 0.125
- down_projection_weight: bfloat16 [2048, 8192], P('sp', 'tp'), may hold values from -0.0625 to 0.0625
Outputs:
- mixed: bfloat16 [12288, 2048], P('sp', 'tp')
All inputs are finite; a program needn't handle non-finite values.
Results may differ from a plain program's by a relative error of at most 0.018.
Values may be sent and summed in bfloat16 or wider, within the bound.
No kernel may reach another device: no remote copies, remote signals or barrier semaphores. Data moves between devices by JAX's collectives and lax.ppermute only.
A program may use at most 128 MiB of HBM per device.

v0:
```python
import functools

import jax
import jax.numpy as jnp
from jax import lax
from jax.experimental import pallas as pl
from jax.experimental.pallas import tpu as pltpu
from jax.sharding import PartitionSpec as P


HEAD_DIM = 64
STATE = 128
BLOCK = 128
MAX_DOCUMENT = 6144
LOG2E = 1.4426950408889634
SIDE = 4

exact_prec = lax.Precision.HIGHEST
norm_eps = 1e-05
resid_scale = 1.4142135623730951
f32 = jnp.float32
bf16 = jnp.bfloat16


SP = ("outer", "inner")


def shifted(array, by, axis=SP):
    count = lax.axis_size(axis)
    pairs = [(i, i + by) for i in range(count) if 0 <= i + by < count]
    return lax.ppermute(array, axis, pairs)


def together(*trees):
    return lax.optimization_barrier(trees)


def partner(array, turn):
    return lax.ppermute(array, "inner", [(i, i ^ turn) for i in range(lax.axis_size("inner"))])


def over_tp(array):
    count = lax.axis_size("tp")
    if count == 1:
        return [array]
    return [array, lax.ppermute(array, "tp", [(0, 1), (1, 0)])]


def columns_over_tp(array):
    count = lax.axis_size("tp")
    if count == 1:
        return array
    if count > 2:
        return lax.all_gather(array, "tp", axis=1, tiled=True)
    own, other = over_tp(array)
    width = array.shape[1]
    place = lax.axis_index("tp")
    joined = jnp.zeros((array.shape[0], 2 * width), array.dtype)
    joined = lax.dynamic_update_slice_in_dim(joined, own, place * width, axis=1)
    return lax.dynamic_update_slice_in_dim(joined, other, (1 - place) * width, axis=1)


def own_columns(array):
    width = array.shape[1] // lax.axis_size("tp")
    return lax.dynamic_slice_in_dim(array, lax.axis_index("tp") * width, width, axis=1)


def scattered(array):
    count = lax.axis_size("tp")
    if count > 2:
        return lax.psum_scatter(array, "tp", scatter_dimension=1, tiled=True).astype(f32)
    if count == 1:
        return array.astype(f32)
    width = array.shape[1] // 2
    place = lax.axis_index("tp")
    away = lax.dynamic_slice_in_dim(array, (1 - place) * width, width, axis=1)
    here = lax.ppermute(away, "tp", [(0, 1), (1, 0)])
    return own_columns(array).astype(f32) + here.astype(f32)


def swap_start(weight):
    count = lax.axis_size("inner")
    place = lax.axis_index("inner")
    width = weight.shape[1] // count
    pieces = []
    for turn in range(count):
        piece = lax.dynamic_slice_in_dim(weight, (place ^ turn) * width, width, axis=1)
        pieces.append(partner(piece, turn) if turn else piece)
    return pieces


def swap_finish(pieces):
    place = lax.axis_index("inner")
    rows, width = pieces[0].shape
    joined = jnp.zeros((rows * len(pieces), width), pieces[0].dtype)
    for turn, piece in enumerate(pieces):
        joined = lax.dynamic_update_slice_in_dim(joined, piece, (place ^ turn) * rows, axis=0)
    return joined


def sum_tp(pair):
    if lax.axis_size("tp") == 2:
        return pair + lax.ppermute(pair, "tp", [(0, 1), (1, 0)])
    return lax.psum(pair, "tp")


def norm_scattered(added, residual, gain):
    total = resid_scale * residual.astype(f32) + added
    width = total.shape[1] * lax.axis_size("tp")
    sums = sum_tp(jnp.stack([jnp.sum(total, axis=1), jnp.sum(total * total, axis=1)]))
    mean = sums[0] / width
    variance = sums[1] / width - mean * mean
    return ((total - mean[:, None]) * lax.rsqrt(variance + norm_eps)[:, None] * gain).astype(bf16)


def spread(columns, heads_per):
    rows = columns.shape[0]
    lane = lax.broadcasted_iota(jnp.int32, (rows, 2 * HEAD_DIM), 1)
    pieces = []
    for pair in range(heads_per // 2):
        low = columns[:, 2 * pair : 2 * pair + 1]
        high = columns[:, 2 * pair + 1 : 2 * pair + 2]
        pieces.append(jnp.where(lane < HEAD_DIM, low, high))
    return jnp.concatenate(pieces, axis=1)


def mixer_kernel(
    value_ref, entry_ref, readout_ref,
    low_value_ref, low_entry_ref, low_readout_ref,
    high_value_ref, high_entry_ref, high_readout_ref,
    value_tap_ref, entry_tap_ref, readout_tap_ref,
    step_ref, sudden_ref, rate_ref, bias_ref, doc_ref, doc_row_ref, *rest,
    first_group,
):
    (out_ref, readout_out_ref, far_ref, end_ref,
     window, values, entries, fresh, starts, cols, lines, sums) = rest[-12:]
    rows, width = value_ref.shape
    per = width // HEAD_DIM
    both = 2 * per
    blocks = rows // BLOCK
    taps = value_tap_ref.shape[0]
    half = taps // 2
    edge = 8
    pieces = [(value_ref, low_value_ref, high_value_ref, value_tap_ref, i * 128, i * 128)
              for i in range(width // 128)]
    pieces.append((entry_ref, low_entry_ref, high_entry_ref, entry_tap_ref, 0, width))
    pieces.append((readout_ref, low_readout_ref, high_readout_ref, readout_tap_ref, 0, width + 128))
    for source, low, high, _, at, to in pieces:
        window[0:edge, to : to + 128] = low[:, at : at + 128].astype(f32)
        window[edge + rows : 2 * edge + rows, to : to + 128] = high[:, at : at + 128].astype(f32)
        window[edge : edge + rows, to : to + 128] = source[:, at : at + 128].astype(f32)

    heads = step_ref.shape[1]
    head = lax.broadcasted_iota(jnp.int32, (heads, both), 0)
    lane = lax.broadcasted_iota(jnp.int32, (heads, both), 1)
    pick = head == (first_group + pl.program_id(0)) * per + jnp.where(lane < per, lane, lane - per)
    pick = jnp.where(pick, 1.0, 0.0)
    at = lax.broadcasted_iota(jnp.int32, (BLOCK, BLOCK), 0)
    source_at = lax.broadcasted_iota(jnp.int32, (BLOCK, BLOCK), 1)
    lower = jnp.where(at >= source_at, 1.0, 0.0)
    unit = jnp.where(at == source_at, 1.0, 0.0)
    ahead_lane = lax.broadcasted_iota(jnp.int32, (1, both), 1) < per

    def conv_block(b, _):
        start = pl.multiple_of(b * BLOCK, BLOCK)
        here = pl.ds(start, BLOCK)
        docs = doc_ref[pl.ds(start, BLOCK + 2 * edge), :]
        own = docs[edge : edge + BLOCK]
        masks = [
            jnp.where(docs[edge - half + k : edge - half + k + BLOCK] == own, 1.0, 0.0)
            for k in range(taps)
        ]
        raw = jnp.dot(step_ref[here, :].astype(f32), pick, preferred_element_type=f32)
        sudden = jnp.dot(sudden_ref[here, :], pick, precision=exact_prec, preferred_element_type=f32)
        raw = raw + bias_ref[...]
        step = jnp.maximum(raw, 0.0) + jnp.log1p(jnp.exp(-jnp.abs(raw)))
        decay = (sudden - jnp.exp(rate_ref[...]) * step) * LOG2E
        cum = jnp.dot(lower, decay, precision=exact_prec, preferred_element_type=f32)
        total = cum[BLOCK - 1 : BLOCK]
        cum = jnp.where(ahead_lane, cum, total - cum + decay)
        leave = jnp.where(ahead_lane, own[BLOCK - 1 : BLOCK], own[0:1])
        come = jnp.where(ahead_lane, docs[edge - 1 : edge], docs[edge + BLOCK : edge + BLOCK + 1])
        outward = jnp.where(own == leave, jnp.exp2(total - cum) * step, 0.0)
        arrive = jnp.where(own == come, jnp.exp2(cum), 0.0)
        passing = jnp.where(leave == come, jnp.exp2(total), 0.0)
        single = jnp.log2(step[:, :per] + step[:, per:])
        cols[here, 0:both] = cum
        cols[here, both : 2 * both] = arrive
        line = jnp.concatenate([jnp.log2(step) - cum, single, single], axis=1)
        lines[b] = lax.dot_general(
            line, unit, (((0,), (0,)), ((), ())), precision=exact_prec, preferred_element_type=f32
        )
        sums[b, 0:1, 0:both] = total
        sums[b, 1:2, 0:both] = passing
        value_parts = []
        for source, low, high, tap_ref, at, to in pieces:
            around = window[pl.ds(start, BLOCK + 2 * edge), to : to + 128]
            acc = jnp.zeros((BLOCK, 128), f32)
            for k in range(taps):
                moved = around[edge - half + k : edge - half + k + BLOCK]
                term = moved * tap_ref[k : k + 1, at : at + 128].astype(f32)
                if k != half:
                    term = term * masks[k]
                acc = acc + term
            active = 0.5 * acc * (1.0 + jnp.tanh(0.5 * acc))
            if to < width:
                value_parts.append(active)
            elif to == width:
                entry = active.astype(bf16)
            else:
                readout_out_ref[here, :] = active.astype(bf16)
        value = jnp.concatenate(value_parts, axis=1)
        values[here, :] = value.astype(bf16)
        entries[here, :] = entry
        forward = value * spread(outward[:, :per], per)
        backward = value * spread(outward[:, per:], per)
        weighted = jnp.concatenate([forward, backward], axis=1).astype(bf16)
        fresh[b] = lax.dot_general(
            entry, weighted, (((0,), (0,)), ((), ())), preferred_element_type=f32
        )
        return 0

    lax.fori_loop(0, blocks, conv_block, 0)

    prev_doc = doc_ref[edge - 1 : edge, :]
    next_doc = doc_ref[edge + rows : edge + rows + 1, :]
    first_doc = doc_ref[edge : edge + 1, :]
    last_doc = doc_ref[edge + rows - 1 : edge + rows, :]
    totals = [sums[b, 0:1, 0:both] for b in range(blocks)]
    passes = [sums[b, 1:2, 0:both] for b in range(blocks)]
    for b in range(blocks):
        nothing = jnp.zeros((1, both), f32)
        sums[b, 2:3, 0:both] = jnp.where(
            ahead_lane, sum(totals[:b], nothing), sum(totals[b + 1 :], nothing)
        )
    whole = jnp.where(
        jnp.where(ahead_lane, prev_doc, next_doc) == jnp.where(ahead_lane, last_doc, first_doc),
        jnp.exp2(sum(totals[1:], totals[0])), 0.0,
    )
    tail_row = lax.broadcasted_iota(jnp.int32, (16, width), 0)
    for k, order in ((0, range(blocks)), (1, range(blocks - 1, -1, -1))):
        span = slice(k * width, (k + 1) * width)
        state = jnp.zeros((STATE, width), f32)
        for b in order:
            starts[b, :, span] = state.astype(bf16)
            factor = spread(passes[b][:, k * per : (k + 1) * per], per)
            state = state * factor + fresh[b, :, span]
        share = STATE // SIDE
        for q in range(SIDE):
            end_ref[q, k, 0:share] = state[q * share : (q + 1) * share].astype(bf16)
        factor = spread(whole[:, k * per : (k + 1) * per], per)
        coarse = factor.astype(bf16).astype(f32)
        tail = jnp.where(tail_row == 0, coarse, jnp.where(tail_row == 1, factor - coarse, 0.0))
        for q in range(SIDE):
            end_ref[q, k, share : share + 16] = tail.astype(bf16)

    def out_block(b, _):
        start = pl.multiple_of(b * BLOCK, BLOCK)
        here = pl.ds(start, BLOCK)
        own = doc_ref[pl.ds(start + edge, BLOCK), :]
        cum = cols[here, 0:both]
        arrive = cols[here, both : 2 * both]
        beyond = jnp.where(ahead_lane, prev_doc, next_doc)
        far_ref[here, :] = jnp.where(own == beyond, jnp.exp2(cum + sums[b, 2:3, 0:both]), 0.0)
        along = lines[b]
        readout = readout_out_ref[here, :]
        entry = entries[here, :]
        value = values[here, :]
        scores = lax.dot_general(
            readout, entry, (((1,), (1,)), ((), ())), preferred_element_type=f32
        )
        scores = jnp.where(own == doc_row_ref[b], scores, 0.0)
        at = lax.broadcasted_iota(jnp.int32, (BLOCK, BLOCK), 0)
        source_at = lax.broadcasted_iota(jnp.int32, (BLOCK, BLOCK), 1)
        value_lane = lax.broadcasted_iota(jnp.int32, (BLOCK, width), 1)
        weights = []
        spreads = []
        for r in range(per):
            ahead = cum[:, r : r + 1] + along[r : r + 1, :]
            behind = cum[:, per + r : per + r + 1] + along[per + r : per + r + 1, :]
            single = along[both + r : both + r + 1, :]
            power = jnp.where(at > source_at, ahead, jnp.where(at < source_at, behind, single))
            weights.append((scores * jnp.exp2(power)).astype(bf16))
            mine = (value_lane >= r * HEAD_DIM) & (value_lane < (r + 1) * HEAD_DIM)
            spreads.append(jnp.where(mine, value, jnp.zeros_like(value)))
        total = jnp.dot(
            jnp.concatenate(weights, axis=1),
            jnp.concatenate(spreads, axis=0),
            preferred_element_type=f32,
        )
        carried = jnp.dot(readout, starts[b], preferred_element_type=f32)
        total = total + carried[:, 0:width] * spread(arrive[:, :per], per)
        total = total + carried[:, width : 2 * width] * spread(arrive[:, per:], per)
        out_ref[here, :] = total
        return 0

    lax.fori_loop(0, blocks, out_block, 0)


def opened(packed):
    rows = packed.shape[0] - 16
    factor = packed[rows : rows + 1, :].astype(f32) + packed[rows + 1 : rows + 2, :].astype(f32)
    return packed[0:rows, :].astype(f32), factor


def closed(pair):
    state, factor = pair
    tail_row = lax.broadcasted_iota(jnp.int32, (16, state.shape[1]), 0)
    coarse = factor.astype(bf16).astype(f32)
    tail = jnp.where(tail_row == 0, coarse, jnp.where(tail_row == 1, factor - coarse, 0.0))
    return jnp.concatenate([state, tail], axis=0).astype(bf16)


def chained(earlier, later):
    return earlier[0] * later[1] + later[0], earlier[1] * later[1]


def whole_kernel(place_ref, *refs):
    pieces, (ahead_ref, behind_ref, ordered) = refs[:-3], refs[-3:]
    for turn, piece in enumerate(pieces):
        ordered[place_ref[0] ^ turn] = piece[...]
    for k, order, out in ((0, (1, 2, 3), ahead_ref), (1, (2, 1, 0), behind_ref)):
        total = opened(ordered[0 if k == 0 else SIDE - 1, k])
        for j in order:
            total = chained(total, opened(ordered[j, k]))
        out[...] = closed(total)


def arrive_kernel(place_ref, *refs):
    pieces, others, (out_ref, ordered, arrived) = refs[:SIDE], refs[SIDE:-3], refs[-3:]
    for turn, piece in enumerate(pieces):
        ordered[place_ref[0] ^ turn] = piece[...]
    count = len(others) // 2
    width = pieces[0].shape[2]
    for k, order in ((0, range(SIDE)), (1, range(SIDE - 1, -1, -1))):
        total = opened(others[k * count])
        for other in others[k * count + 1 : (k + 1) * count]:
            total = chained(opened(other), total)
        for j in order:
            arrived[j, :, k * width : (k + 1) * width] = total[0].astype(bf16)
            total = chained(total, opened(ordered[j, k]))
    for turn in range(SIDE):
        out_ref[turn] = arrived[place_ref[0] ^ turn]


def gate_kernel(place_ref, *refs):
    mixed_ref, readout_ref, far_ref, gate_ref, gain_ref = refs[:5]
    pieces, out_ref, state_ref = refs[5:-2], refs[-2], refs[-1]
    rows, width = mixed_ref.shape
    per = width // HEAD_DIM
    share = STATE // SIDE
    for turn, piece in enumerate(pieces):
        at = pl.multiple_of((place_ref[0] ^ turn) * share, share)
        state_ref[pl.ds(at, share), :] = piece[...]

    def one(b, _):
        here = pl.ds(pl.multiple_of(b * BLOCK, BLOCK), BLOCK)
        far = far_ref[here, :]
        carried = jnp.dot(readout_ref[here, :], state_ref[...], preferred_element_type=f32)
        total = mixed_ref[here, :]
        total = total + carried[:, 0:width] * spread(far[:, :per], per)
        total = total + carried[:, width : 2 * width] * spread(far[:, per:], per)
        gate = gate_ref[here, :].astype(f32)
        total = total * (0.5 * gate * (1.0 + jnp.tanh(0.5 * gate)))
        scale = lax.rsqrt(jnp.mean(total * total, axis=1, keepdims=True) + norm_eps)
        out_ref[here, :] = (total * scale * gain_ref[...]).astype(bf16)
        return 0

    lax.fori_loop(0, rows // BLOCK, one, 0)


def up_kernel(place_ref, own_ref, other_ref, weight_ref, out_ref, rows_ref):
    depth = own_ref.shape[1]
    outer, wide, tile = weight_ref.shape

    @pl.when(pl.program_id(0) == 0)
    def _():
        place = place_ref[0]
        rows_ref[:, pl.ds(pl.multiple_of(place * depth, depth), depth)] = own_ref[...]
        rows_ref[:, pl.ds(pl.multiple_of((1 - place) * depth, depth), depth)] = other_ref[...]

    weight = weight_ref[...].reshape(outer * wide, tile)
    hidden = jnp.dot(rows_ref[...], weight, preferred_element_type=f32)
    hidden = jnp.maximum(hidden, 0.0)
    out_ref[...] = (hidden * hidden).astype(bf16)


def up_rows(place, own, other, weights):
    rows, depth = own.shape
    outer, wide, units = weights.shape
    tile = units // 2
    return pl.pallas_call(
        up_kernel,
        grid=(units // tile,),
        in_specs=[
            pl.BlockSpec(memory_space=pltpu.SMEM),
            pl.BlockSpec((rows, depth), lambda i: (0, 0)),
            pl.BlockSpec((rows, depth), lambda i: (0, 0)),
            pl.BlockSpec((outer, wide, tile), lambda i: (0, 0, i)),
        ],
        out_specs=pl.BlockSpec((rows, tile), lambda i: (0, i)),
        out_shape=jax.ShapeDtypeStruct((rows, units), bf16),
        scratch_shapes=[pltpu.VMEM((rows, 2 * depth), bf16)],
        name="up_rows",
    )(place, own, other, weights)


def down_kernel(place_ref, *refs):
    pieces, (weight_ref, out_ref) = refs[:-2], refs[-2:]
    at = 0
    for piece in pieces:
        rows = piece.shape[0]
        out_ref[at : at + rows, :] = lax.dot_general(
            piece[...], weight_ref[...], (((1,), (1,)), ((), ())), preferred_element_type=f32
        ).astype(bf16)
        at += rows


def down_rows(place, pieces, weights):
    rows = sum(piece.shape[0] for piece in pieces)
    outer, wide, units = weights.shape
    half = outer // 2
    grid_spec = pltpu.PrefetchScalarGridSpec(
        num_scalar_prefetch=1,
        grid=(outer,),
        in_specs=[pl.BlockSpec(piece.shape, lambda i, place: (0, 0)) for piece in pieces] + [
            pl.BlockSpec(
                (pl.Squeezed(), wide, units),
                lambda i, place: ((i + place[0] * half) % outer, 0, 0),
            )
        ],
        out_specs=pl.BlockSpec(
            (pl.Squeezed(), rows, wide), lambda i, place: (i // half, 0, i % half)
        ),
    )
    return pl.pallas_call(
        down_kernel,
        grid_spec=grid_spec,
        out_shape=jax.ShapeDtypeStruct((2, rows, half * wide), bf16),
        name="down_rows",
    )(place, *pieces, weights)


def norm_kernel(place_ref, *refs):
    parts, (stream_ref, gain_ref, own_ref, other_ref) = refs[:-4], refs[-4:]
    total = resid_scale * stream_ref[...].astype(f32)
    added = parts[0][...].astype(f32)
    for part in parts[1:]:
        added = added + part[...].astype(f32)
    total = total + added
    width = total.shape[1]
    mean = jnp.sum(total, axis=1, keepdims=True) / width
    variance = jnp.sum(total * total, axis=1, keepdims=True) / width - mean * mean
    normed = (total - mean) * lax.rsqrt(variance + norm_eps) * gain_ref[...]
    left, right = normed[:, : width // 2], normed[:, width // 2 :]
    first = place_ref[0] == 0
    own_ref[...] = jnp.where(first, left, right).astype(bf16)
    other_ref[...] = jnp.where(first, right, left).astype(bf16)


def norm_rows(place, parts, stream, gain):
    rows, width = stream.shape
    tile = min(rows, BLOCK)
    spec = pl.BlockSpec((tile, width), lambda i: (i, 0))
    half_spec = pl.BlockSpec((tile, width // 2), lambda i: (i, 0))
    return pl.pallas_call(
        norm_kernel,
        grid=(rows // tile,),
        in_specs=[pl.BlockSpec(memory_space=pltpu.SMEM)] + [spec] * (len(parts) + 1)
        + [pl.BlockSpec((1, width), lambda i: (0, 0))],
        out_specs=[half_spec] * 2,
        out_shape=[jax.ShapeDtypeStruct((rows, width // 2), bf16)] * 2,
        name="norm_rows",
    )(place, *parts, stream, gain)


def per_device(
    head_value_rows,
    entry_map_rows,
    readout_map_rows,
    output_gate_rows,
    step_before_softplus,
    sudden_log_decay,
    document_index,
    head_rate_logarithm,
    head_step_bias,
    value_conv_taps,
    entry_conv_taps,
    readout_conv_taps,
    group_norm_gain,
    mixer_output_weight,
    stream,
    mixer_norm_gain,
    channel_norm_gain,
    up_projection_weight,
    down_projection_weight,
):
    row_count = head_value_rows.shape[0]
    head_count = step_before_softplus.shape[1]
    groups = entry_map_rows.shape[1] // STATE
    per = head_count // groups
    width = per * HEAD_DIM
    blocks = row_count // BLOCK
    taps = value_conv_taps.shape[0]
    edge = 8

    joined_low = jnp.concatenate(
        [a[-edge:] for a in (head_value_rows, entry_map_rows, readout_map_rows)], axis=1
    )
    joined_high = jnp.concatenate(
        [a[:edge] for a in (head_value_rows, entry_map_rows, readout_map_rows)], axis=1
    )
    low = shifted(joined_low, 1)
    high = shifted(joined_high, -1)
    up_swaps = swap_start(up_projection_weight)
    (low, high), up_swaps, down_own = together((low, high), up_swaps, down_projection_weight)
    up_weights = lax.all_gather(swap_finish(up_swaps), "outer")
    down_swaps = swap_start(down_own)

    position = lax.axis_index(SP) * row_count
    doc_pad = jnp.pad(document_index, edge, constant_values=-1)
    around = lax.dynamic_slice_in_dim(doc_pad, position, row_count + 2 * edge).astype(f32)
    doc_column = around[:, None]
    doc_rows = around[edge : edge + row_count].reshape(blocks, 1, BLOCK)

    def lanes(array):
        return array.reshape(2, groups, per).transpose(1, 0, 2).reshape(groups, 1, 2 * per)

    def rows_spec(columns_wide, first=0):
        return pl.BlockSpec((row_count, columns_wide), lambda g: (0, first + g))

    def thin_spec(height, columns_wide, first=0):
        return pl.BlockSpec((height, columns_wide), lambda g: (0, first + g))

    def group_spec(*shape, first=0):
        return pl.BlockSpec(
            (pl.Squeezed(),) + shape, lambda g: (first + g,) + (0,) * len(shape)
        )

    def same_spec(*shape):
        return pl.BlockSpec(shape, lambda g: (0,) * len(shape))

    value_width, map_width = groups * width, groups * STATE
    share = STATE // SIDE
    pack_rows = share + 16

    def mixer(first, count, so_far):
        edge_specs = [
            thin_spec(edge, width, first),
            thin_spec(edge, STATE, value_width // STATE + first),
            thin_spec(edge, STATE, (value_width + map_width) // STATE + first),
        ]
        given = [
            head_value_rows, entry_map_rows, readout_map_rows, low, low, low, high, high, high,
            value_conv_taps, entry_conv_taps, readout_conv_taps, step_before_softplus,
            sudden_log_decay, lanes(head_rate_logarithm), lanes(head_step_bias), doc_column, doc_rows,
        ]
        return pl.pallas_call(
            functools.partial(mixer_kernel, first_group=first),
            grid=(count,),
            in_specs=[
                rows_spec(width, first), rows_spec(STATE, first), rows_spec(STATE, first),
                *edge_specs, *edge_specs,
                thin_spec(taps, width, first), thin_spec(taps, STATE, first),
                thin_spec(taps, STATE, first),
                same_spec(row_count, head_count), same_spec(row_count, head_count),
                group_spec(1, 2 * per, first=first), group_spec(1, 2 * per, first=first),
                same_spec(row_count + 2 * edge, 1), same_spec(blocks, 1, BLOCK),
            ] + [pl.BlockSpec(memory_space=pl.ANY)] * len(so_far),
            out_specs=[
                rows_spec(width, first), rows_spec(STATE, first),
                group_spec(row_count, 2 * per, first=first),
                pl.BlockSpec(
                    (SIDE, 2, pl.Squeezed(), pack_rows, width), lambda g: (0, 0, first + g, 0, 0)
                ),
            ],
            out_shape=[
                jax.ShapeDtypeStruct((row_count, groups * width), f32),
                jax.ShapeDtypeStruct((row_count, groups * STATE), bf16),
                jax.ShapeDtypeStruct((groups, row_count, 2 * per), f32),
                jax.ShapeDtypeStruct((SIDE, 2, groups, pack_rows, width), bf16),
            ],
            input_output_aliases={len(given) + i: i for i in range(len(so_far))},
            scratch_shapes=[
                pltpu.VMEM((row_count + 2 * edge, width + 2 * STATE), f32),
                pltpu.VMEM((row_count, width), bf16),
                pltpu.VMEM((row_count, STATE), bf16),
                pltpu.VMEM((blocks, STATE, 2 * width), f32),
                pltpu.VMEM((blocks, STATE, 2 * width), bf16),
                pltpu.VMEM((row_count, 128), f32),
                pltpu.VMEM((blocks, 4 * per, BLOCK), f32),
                pltpu.VMEM((blocks, 8, 128), f32),
            ],
            name="mixer",
        )(*given, *so_far)

    local, readouts, far, ends = mixer(0, groups, [])

    reach = min(lax.axis_size(SP) - 1, -(-(MAX_DOCUMENT - 1) // row_count))
    spans = -(-reach // SIDE)
    inner_place = lax.axis_index("inner").astype(jnp.int32)[None]

    def share_of(array, turn):
        return lax.dynamic_index_in_dim(array, lax.axis_index("inner") ^ turn, 0, keepdims=False)

    shares = [share_of(ends, 0)] + [partner(share_of(ends, turn), turn) for turn in (1, 2, 3)]
    smem = pl.BlockSpec(memory_space=pltpu.SMEM)
    share_spec = pl.BlockSpec((2, pl.Squeezed(), pack_rows, width), lambda g: (0, g, 0, 0))
    pack_spec = group_spec(pack_rows, width)
    pack_shape = jax.ShapeDtypeStruct((groups, pack_rows, width), bf16)
    ordered = pltpu.VMEM((SIDE, 2, pack_rows, width), bf16)
    ahead, behind = pl.pallas_call(
        whole_kernel,
        grid=(groups,),
        in_specs=[smem] + [share_spec] * SIDE,
        out_specs=[pack_spec] * 2,
        out_shape=[pack_shape] * 2,
        scratch_shapes=[ordered],
        name="whole",
    )(inner_place, *shares)
    others = [shifted(ahead, j, "outer") for j in range(1, spans + 1)]
    others = others + [shifted(behind, -j, "outer") for j in range(1, spans + 1)]
    arrivals = pl.pallas_call(
        arrive_kernel,
        grid=(groups,),
        in_specs=[smem] + [share_spec] * SIDE + [pack_spec] * len(others),
        out_specs=pl.BlockSpec((SIDE, pl.Squeezed(), share, 2 * width), lambda g: (0, g, 0, 0)),
        out_shape=jax.ShapeDtypeStruct((SIDE, groups, share, 2 * width), bf16),
        scratch_shapes=[ordered, pltpu.VMEM((SIDE, share, 2 * width), bf16)],
        name="arrive",
    )(inner_place, *shares, *others)
    packs = [arrivals[0]] + [partner(arrivals[turn], turn) for turn in (1, 2, 3)]
    down_weights = lax.all_gather(swap_finish(down_swaps), "outer")

    tp_count = lax.axis_size("tp")
    if tp_count == 2:
        stream_full = columns_over_tp(stream)
        gain_one = columns_over_tp(mixer_norm_gain[None])
        packs, stream_full, gain_one = together(packs, stream_full, gain_one)
    normed = pl.pallas_call(
        gate_kernel,
        grid=(groups,),
        in_specs=[
            smem, rows_spec(width), rows_spec(STATE), group_spec(row_count, 2 * per),
            rows_spec(width), thin_spec(1, width),
        ] + [group_spec(share, 2 * width)] * SIDE,
        out_specs=rows_spec(width),
        out_shape=jax.ShapeDtypeStruct((row_count, groups * width), bf16),
        scratch_shapes=[pltpu.VMEM((STATE, 2 * width), bf16)],
        name="gate",
    )(inner_place, local, readouts, far, output_gate_rows, group_norm_gain[None], *packs)

    part = jnp.dot(normed, mixer_output_weight, preferred_element_type=f32).astype(bf16)
    place = lax.axis_index("tp").astype(jnp.int32)[None]
    if tp_count == 2:
        own_one, other_one = norm_rows(place, over_tp(part), stream_full, gain_one)
    else:
        own_one = norm_scattered(scattered(part), stream, mixer_norm_gain)
        other_one = None

    def hidden_units(rows, other=None):
        if tp_count == 2:
            other = over_tp(rows)[1] if other is None else other
            return up_rows(place, rows, other, up_weights)
        up = up_weights.reshape(-1, up_weights.shape[2])
        hidden = jnp.dot(columns_over_tp(rows), up, preferred_element_type=f32)
        return jnp.square(jax.nn.relu(hidden)).astype(bf16)

    def contributions(pieces):
        if tp_count == 2:
            both = down_rows(place, pieces, down_weights)
            other = lax.ppermute(both[1], "tp", [(0, 1), (1, 0)])
            return (both[0].astype(f32) + other.astype(f32)).astype(bf16)
        down = down_weights.reshape(-1, down_weights.shape[2])
        product = lax.dot_general(
            jnp.concatenate(pieces, axis=0), down, (((1,), (1,)), ((), ())),
            preferred_element_type=f32,
        )
        return scattered(product.astype(bf16)).astype(bf16)

    middle = row_count // 2
    side_one, side_two = partner(own_one, 1), partner(own_one, 2)
    units = hidden_units(own_one, other_one)
    side_one, side_two, units = together(side_one, side_two, units)
    far_one = partner(side_one[:middle], 2)
    far_two = partner(side_two[middle:], 1)
    near_units = [units, hidden_units(side_one), hidden_units(side_two)]
    near = contributions(near_units)
    far_rows = [far_one, far_two]
    near, far_rows = together(near, far_rows)
    back_one = partner(near[row_count : 2 * row_count], 1)
    back_two = partner(near[2 * row_count :], 2)
    diagonal_units = [hidden_units(rows) for rows in far_rows]
    diagonal = contributions(diagonal_units)
    first_hop = [partner(diagonal[:middle], 2), partner(diagonal[middle:], 1)]
    second_hop = [partner(first_hop[0], 1), partner(first_hop[1], 2)]
    added = near[:row_count].astype(f32) + back_one.astype(f32) + back_two.astype(f32)
    added = added + jnp.concatenate(second_hop, axis=0).astype(f32)
    return norm_scattered(added, own_one, channel_norm_gain)


def solution(mesh):
    sp_count, tp_count = mesh.devices.shape
    inner = SIDE
    finer = jax.sharding.Mesh(
        mesh.devices.reshape(sp_count // inner, inner, tp_count), ("outer", "inner", "tp")
    )
    both = P(SP, "tp")
    second = P(None, "tp")
    placed = (
        both, both, both, both, both, both, P(), second, second, second, second, second,
        P("tp"), P("tp", None), both, P("tp"), P("tp"), both, both,
    )
    return jax.shard_map(
        per_device, mesh=finer, in_specs=placed, out_specs=both, check_vma=False
    )
```

profile of v0, /device:TPU:0, one launch (start us, length us, event | category | flops | bytes accessed | tf_op | source)
XLA Modules:
  0.0 379.5 jit_solution(2838952239977292129)
XLA Ops:
  7.9 4.0 %collective-permute-start.4 = (bf16[128,1024]{1,0:T(8,128)(2,1)S(1)}, bf16[128,1024]{1,0:T(8,128)(2,1)S(1)}, u32[]{:S(2)}, u32[]{:S(2)}) collective-permute-start(bf16[128,1024]{1,0:T(8,128)(2,1)S(1)} %get-tuple-element.73), channel_id=1, source_target_pairs={{0,6},{2,4},{4,2},{6,0},{1,7},{3,5},{5,3},{7,1},{8,14},{10,12},{12... | collective-permute-start | bytes 786440 | tf_op jit(solution)/shard_map/ppermute | solution.py:39
  14.0 3.8 collective-permute-start
  19.1 5.0 %collective-permute-done.low_value_ref.low_entry_ref.low_readout_ref = bf16[8,2048]{1,0:T(8,128)(2,1)S(1)} collective-permute-done((bf16[8,2048]{1,0:T(8,128)(2,1)S(1)}, bf16[8,2048]{1,0:T(8,128)(2,1)S(1)}, u32[]{:S(2)}, u32[]{:S(2)}) %collective-permute-start) | collective-permute-done | bytes 32800 | tf_op jit(solution)/shard_map/ppermute | solution.py:31
  32.7 1.8 constant_dynamic-update-slice_fusion.3
  36.8 41.0 %mixer.1 = (f32[768,1024]{1,0:T(8,128)}, bf16[768,512]{1,0:T(8,128)(2,1)}, f32[4,768,8]{2,1,0:T(8,128)}, bf16[4,2,4,48,256]{4,3,2,1,0:T(8,128)(2,1)}) custom-call(bf16[768,1024]{1,0:T(8,128)(2,1)} %value_ref.1, bf16[768,512]{1,0:T(8,128)(2,1)} %entry_ref.1, bf16[768,512]{1,0:T(8,128)(2,1)} %readout_ref.1, bf16[8,2048]{1,0:T(8,128)(2,1)} %copy-done.17, ...), custom_call_target="tpu_custom_call" | custom-call | tf_op jit(solution)/shard_map/mixer/pallas_call | solution.py:558
  77.9 2.1 dynamic-slice_bitcast_fusion
  83.6 5.3 %collective-permute-done.7.refs_3_ = bf16[2,4,48,256]{3,2,1,0:T(8,128)(2,1)S(1)} collective-permute-done((bf16[2,4,48,256]{3,2,1,0:T(8,128)(2,1)}, bf16[2,4,48,256]{3,2,1,0:T(8,128)(2,1)S(1)}, u32[]{:S(2)}, u32[]{:S(2)}) %collective-permute-start.7) | collective-permute-done | bytes 196640 | tf_op jit(solution)/shard_map/ppermute | solution.py:39
  88.9 1.6 collective-permute-start.23
  91.6 1.7 bitcast_dynamic-update-slice_fusion.3
  94.0 3.1 whole.1
  97.1 4.5 %collective-permute-start.9 = (bf16[4,48,256]{2,1,0:T(8,128)(2,1)}, bf16[4,48,256]{2,1,0:T(8,128)(2,1)S(1)}, u32[]{:S(2)}, u32[]{:S(2)}) collective-permute-start(bf16[4,48,256]{2,1,0:T(8,128)(2,1)} %get-tuple-element.38), channel_id=1, source_target_pairs={{0,16},{8,24},{1,17},{9,25},{2,18},{10,26},{3,19},{11,27},{4,20},{... | collective-permute-start | bytes 294920 | tf_op jit(solution)/shard_map/ppermute | solution.py:31
  101.5 3.0 collective-permute-start.8
  105.9 1.7 bitcast_dynamic-update-slice_fusion.2
  109.0 1.7 bitcast_dynamic-update-slice_fusion.1
  110.7 1.8 collective-permute-start.24
  112.9 2.0 collective-permute-done.10.refs_6_
  114.9 3.3 arrive.1
  118.2 1.8 slice_bitcast_fusion.4
  119.9 1.6 collective-permute-start.14
  123.4 1.6 constant_dynamic-update-slice_fusion.2.refs_2_
  125.1 2.1 collective-permute-done.14.refs_8_
  127.1 1.6 collective-permute-done.13.refs_7_
  128.7 10.3 %gate.1 = bf16[768,1024]{1,0:T(8,128)(2,1)} custom-call(s32[1]{0:T(128)} %bitcast.1.place_ref, f32[768,1024]{1,0:T(8,128)} %get-tuple-element.34.refs_0_, bf16[768,512]{1,0:T(8,128)(2,1)} %get-tuple-element.35.refs_1_, f32[4,768,8]{2,1,0:T(8,128)} %get-tuple-element.36.refs_2_, bf16[768,1024]{1,0:T(8,128)(2,1)} %refs_3_.1, f32[1,1024]{1,0:T(1,128)} %bitcast.60, ...), custom_call_target="tpu_custom_call" | custom-call | tf_op jit(solution)/shard_map/gate/pallas_call | solution.py:640
  139.0 7.7 %convolution_convert_fusion.refs_0_ = bf16[768,2048]{1,0:T(8,128)(2,1)} fusion(bf16[768,1024]{1,0:T(8,128)(2,1)} %gate.1, bf16[1024,2048]{1,0:T(8,128)(2,1)} %param.32), kind=kOutput, calls=%fused_computation.4 | convolution fusion | flops 3222798336 | bytes 8912896 | tf_op jit(solution)/shard_map/dot_general | solution.py:653
  147.5 5.1 %collective-permute-done.17.refs_1_ = bf16[768,2048]{1,0:T(8,128)(2,1)S(1)} collective-permute-done((bf16[768,2048]{1,0:T(8,128)(2,1)}, bf16[768,2048]{1,0:T(8,128)(2,1)S(1)}, u32[]{:S(2)}, u32[]{:S(2)}) %collective-permute-start.17) | collective-permute-done | bytes 3145760 | tf_op jit(solution)/shard_map/ppermute | solution.py:46
  152.6 1.7 copy-done.9
  154.3 8.4 %norm_rows.1 = (bf16[768,1024]{1,0:T(8,128)(2,1)}, bf16[768,1024]{1,0:T(8,128)(2,1)}) custom-call(s32[1]{0:T(128)} %bitcast.place_ref, bf16[768,2048]{1,0:T(8,128)(2,1)} %convolution_convert_fusion.refs_0_, bf16[768,2048]{1,0:T(8,128)(2,1)} %copy-done.9, bf16[768,2048]{1,0:T(8,128)(2,1)} %copy-done.2, f32[1,2048]{1,0:T(1,128)} %copy-done.23), custom_call_target="tpu_custom_call" | custom-call | tf_op jit(solution)/shard_map/norm_rows/pallas_call | solution.py:466
  164.7 7.3 %up_rows.5.refs_0_ = bf16[768,1024]{1,0:T(8,128)(2,1)} custom-call(s32[1]{0:T(128)} %bitcast.place_ref, bf16[768,1024]{1,0:T(8,128)(2,1)} %get-tuple-element.46.own_ref, bf16[768,1024]{1,0:T(8,128)(2,1)} %get-tuple-element.47.other_ref, bf16[4,512,1024]{2,1,0:T(8,128)(2,1)} %all-gather.3.cloned.1.call-done.weight_ref), custom_call_target="tpu_custom_call" | custom-call | tf_op jit(solution)/shard_map/up_rows/pallas_call | solution.py:392
  172.0 27.3 %collective-permute-done.19.own_ref = bf16[768,1024]{1,0:T(8,128)(2,1)S(1)} collective-permute-done((bf16[768,1024]{1,0:T(8,128)(2,1)}, bf16[768,1024]{1,0:T(8,128)(2,1)S(1)}, u32[]{:S(2)}, u32[]{:S(2)}) %collective-permute-start.19) | collective-permute-done | bytes 1572896 | tf_op jit(solution)/shard_map/ppermute | solution.py:39
  200.1 3.0 collective-permute-done.20.other_ref
  203.1 7.2 %up_rows.6.refs_1_ = bf16[768,1024]{1,0:T(8,128)(2,1)} custom-call(s32[1]{0:T(128)} %bitcast.place_ref, bf16[768,1024]{1,0:T(8,128)(2,1)} %copy-done.7, bf16[768,1024]{1,0:T(8,128)(2,1)} %collective-permute-done.20.other_ref, bf16[4,512,1024]{2,1,0:T(8,128)(2,1)} %all-gather.3.cloned.1.call-done.weight_ref), custom_call_target="tpu_custom_call" | custom-call | tf_op jit(solution)/shard_map/up_rows/pallas_call | solution.py:392
  210.4 7.3 %up_rows.7.refs_2_ = bf16[768,1024]{1,0:T(8,128)(2,1)} custom-call(s32[1]{0:T(128)} %bitcast.place_ref, bf16[768,1024]{1,0:T(8,128)(2,1)} %copy-done.5, bf16[768,1024]{1,0:T(8,128)(2,1)} %collective-permute-done.21.other_ref, bf16[4,512,1024]{2,1,0:T(8,128)(2,1)} %all-gather.3.cloned.1.call-done.weight_ref), custom_call_target="tpu_custom_call" | custom-call | tf_op jit(solution)/shard_map/up_rows/pallas_call | solution.py:392
  217.6 10.6 %all-gather.5.cloned.1.call-done.refs_3_.refs_2_ = bf16[4,512,1024]{2,1,0:T(8,128)(2,1)} async-done(((bf16[1,512,1024]{2,1,0:T(8,128)(2,1)}), bf16[4,512,1024]{2,1,0:T(8,128)(2,1)}) %all-gather.5.cloned.1.call-update) | async-done | bytes 4194320 | tf_op jit(solution)/shard_map/all_gather | solution.py:633
  228.2 15.0 %down_rows.2 = bf16[2,2304,1024]{2,1,0:T(8,128)(2,1)} custom-call(s32[1]{0:T(128)} %bitcast.place_ref, bf16[768,1024]{1,0:T(8,128)(2,1)} %up_rows.5.refs_0_, bf16[768,1024]{1,0:T(8,128)(2,1)} %up_rows.6.refs_1_, bf16[768,1024]{1,0:T(8,128)(2,1)} %up_rows.7.refs_2_, bf16[4,512,1024]{2,1,0:T(8,128)(2,1)} %all-gather.5.cloned.1.call-done.refs_3_.refs_2_), custom_call_target="tpu_custom_call" | custom-call | tf_op jit(solution)/shard_map/down_rows/pallas_call | solution.py:436
  243.2 3.0 slice_bitcast_fusion
  246.5 1.5 collective-permute-start.27
  249.5 4.7 %collective-permute-done.25 = bf16[2304,1024]{1,0:T(8,128)(2,1)S(1)} collective-permute-done((bf16[2304,1024]{1,0:T(8,128)(2,1)S(1)}, bf16[2304,1024]{1,0:T(8,128)(2,1)S(1)}, u32[]{:S(2)}, u32[]{:S(2)}) %collective-permute-start.25) | collective-permute-done | bytes 4718624 | tf_op jit(solution)/shard_map/ppermute | solution.py:672
  254.2 4.7 %fusion = bf16[2304,1024]{1,0:T(8,128)(2,1)} fusion(bf16[2304,1024]{1,0:T(8,128)(2,1)S(1)} %collective-permute-done.25, bf16[2,2304,1024]{2,1,0:T(8,128)(2,1)S(1)} %copy-done), kind=kLoop, calls=%fused_computation.1 | loop fusion | flops 9437184 | bytes 14155776 | tf_op jit(solution)/shard_map/convert_element_type | solution.py:673
  258.9 7.5 %collective-permute-done.27.own_ref = bf16[384,1024]{1,0:T(8,128)(2,1)S(1)} collective-permute-done((bf16[384,1024]{1,0:T(8,128)(2,1)S(1)}, bf16[384,1024]{1,0:T(8,128)(2,1)S(1)}, u32[]{:S(2)}, u32[]{:S(2)}) %collective-permute-start.27) | collective-permute-done | bytes 786464 | tf_op jit(solution)/shard_map/ppermute | solution.py:39
  268.2 1.8 collective-permute-done.30.other_ref
  270.9 4.9 %up_rows.8.refs_0_ = bf16[384,1024]{1,0:T(8,128)(2,1)} custom-call(s32[1]{0:T(128)} %bitcast.place_ref, bf16[384,1024]{1,0:T(8,128)(2,1)} %copy-done.14, bf16[384,1024]{1,0:T(8,128)(2,1)} %copy-done.16, bf16[4,512,1024]{2,1,0:T(8,128)(2,1)} %all-gather.3.cloned.1.call-done.weight_ref), custom_call_target="tpu_custom_call" | custom-call | tf_op jit(solution)/shard_map/up_rows/pallas_call | solution.py:392
  276.6 4.9 %up_rows.9.refs_1_ = bf16[384,1024]{1,0:T(8,128)(2,1)} custom-call(s32[1]{0:T(128)} %bitcast.place_ref, bf16[384,1024]{1,0:T(8,128)(2,1)} %copy-done.13, bf16[384,1024]{1,0:T(8,128)(2,1)} %copy-done.15, bf16[4,512,1024]{2,1,0:T(8,128)(2,1)} %all-gather.3.cloned.1.call-done.weight_ref), custom_call_target="tpu_custom_call" | custom-call | tf_op jit(solution)/shard_map/up_rows/pallas_call | solution.py:392
  281.5 7.4 %down_rows.3 = bf16[2,768,1024]{2,1,0:T(8,128)(2,1)} custom-call(s32[1]{0:T(128)} %bitcast.place_ref, bf16[384,1024]{1,0:T(8,128)(2,1)} %up_rows.8.refs_0_, bf16[384,1024]{1,0:T(8,128)(2,1)} %up_rows.9.refs_1_, bf16[4,512,1024]{2,1,0:T(8,128)(2,1)} %all-gather.5.cloned.1.call-done.refs_3_.refs_2_), custom_call_target="tpu_custom_call" | custom-call | tf_op jit(solution)/shard_map/down_rows/pallas_call | solution.py:436
  290.6 2.3 fusion.7
  298.0 48.9 %collective-permute-done.33 = bf16[384,1024]{1,0:T(8,128)(2,1)S(1)} collective-permute-done((bf16[384,1024]{1,0:T(8,128)(2,1)S(1)}, bf16[384,1024]{1,0:T(8,128)(2,1)S(1)}, u32[]{:S(2)}, u32[]{:S(2)}) %collective-permute-start.33) | collective-permute-done | bytes 786464 | tf_op jit(solution)/shard_map/ppermute | solution.py:39
  349.9 15.8 %collective-permute-done.34 = bf16[384,1024]{1,0:T(8,128)(2,1)S(1)} collective-permute-done((bf16[384,1024]{1,0:T(8,128)(2,1)S(1)}, bf16[384,1024]{1,0:T(8,128)(2,1)S(1)}, u32[]{:S(2)}, u32[]{:S(2)}) %collective-permute-start.34) | collective-permute-done | bytes 786464 | tf_op jit(solution)/shard_map/ppermute | solution.py:39
  366.9 2.8 fusion.6
  371.1 1.6 multiply_convert_fusion
  (157 shorter events, 46.7 us)
Async XLA Ops:
  6.5 158.1 %all-gather.3.cloned.1.call-start = ((), (), s32[]{:S(2)}) async-start(), calls=%async_computation | async-start | bytes 5242880 | tf_op jit(solution)/shard_map/all_gather | solution.py:517
  6.5 20.9 %copy-start.22 = (s32[12288]{0:T(1024)S(1)}, s32[12288]{0:T(1024)}, u32[]{:S(2)}) copy-start(s32[12288]{0:T(1024)} %param.25) | copy-start | bytes 147460
  6.5 22.6 %copy-start.27 = (f32[2,16]{1,0:T(2,128)S(1)}, f32[2,16]{1,0:T(2,128)}, u32[]{:S(2)}) copy-start(f32[2,16]{1,0:T(2,128)} %param.26) | copy-start | bytes 388
  6.5 23.3 %copy-start.28 = (f32[2,16]{1,0:T(2,128)S(1)}, f32[2,16]{1,0:T(2,128)}, u32[]{:S(2)}) copy-start(f32[2,16]{1,0:T(2,128)} %param.27) | copy-start | bytes 388
  6.5 24.1 %copy-start.24 = (bf16[768,16]{0,1:T(8,128)(2,1)S(1)}, bf16[768,16]{0,1:T(8,128)(2,1)}, u32[]{:S(2)}) copy-start(bf16[768,16]{0,1:T(8,128)(2,1)} %param.23) | copy-start | bytes 73732
  7.9 23.5 %copy-start.21 = (f32[768,16]{0,1:T(8,128)S(1)}, f32[768,16]{0,1:T(8,128)}, u32[]{:S(2)}) copy-start(f32[768,16]{0,1:T(8,128)} %param.24) | copy-start | bytes 147460
  7.9 17.6 %collective-permute-start.4 = (bf16[128,1024]{1,0:T(8,128)(2,1)S(1)}, bf16[128,1024]{1,0:T(8,128)(2,1)S(1)}, u32[]{:S(2)}, u32[]{:S(2)}) collective-permute-start(bf16[128,1024]{1,0:T(8,128)(2,1)S(1)} %get-tuple-element.73), channel_id=1, source_target_pairs={{0,6},{2,4},{4,2},{6,0},{1,7},{3,5},{5,3},{7,1},{8,14},{10,12},{12... | collective-permute-start | bytes 786440 | tf_op jit(solution)/shard_map/ppermute | solution.py:39
  11.9 13.6 %collective-permute-start.2 = (bf16[128,1024]{1,0:T(8,128)(2,1)S(1)}, bf16[128,1024]{1,0:T(8,128)(2,1)S(1)}, u32[]{:S(2)}, u32[]{:S(2)}) collective-permute-start(bf16[128,1024]{1,0:T(8,128)(2,1)S(1)} %get-tuple-element.74), channel_id=1, source_target_pairs={{0,2},{2,0},{4,6},{6,4},{1,3},{3,1},{5,7},{7,5},{8,10},{10,8},{12,... | collective-permute-start | bytes 786440 | tf_op jit(solution)/shard_map/ppermute | solution.py:39
  12.4 13.1 %collective-permute-start.3 = (bf16[128,1024]{1,0:T(8,128)(2,1)S(1)}, bf16[128,1024]{1,0:T(8,128)(2,1)S(1)}, u32[]{:S(2)}, u32[]{:S(2)}) collective-permute-start(bf16[128,1024]{1,0:T(8,128)(2,1)S(1)} %get-tuple-element.76), channel_id=1, source_target_pairs={{0,4},{2,6},{4,0},{6,2},{1,5},{3,7},{5,1},{7,3},{8,12},{10,14},{12... | collective-permute-start | bytes 786440 | tf_op jit(solution)/shard_map/ppermute | solution.py:39
  14.0 10.1 %collective-permute-start = (bf16[8,2048]{1,0:T(8,128)(2,1)S(1)}, bf16[8,2048]{1,0:T(8,128)(2,1)S(1)}, u32[]{:S(2)}, u32[]{:S(2)}) collective-permute-start(bf16[8,2048]{1,0:T(8,128)(2,1)S(1)} %pad_maximum_fusion), channel_id=1, source_target_pairs={{0,2},{2,4},{4,6},{6,8},{8,10},{10,12},{12,14},{14,16},{16,18},{18... | collective-permute-start | bytes 98312 | tf_op jit(solution)/shard_map/ppermute | solution.py:31
  17.8 7.7 %collective-permute-start.1 = (bf16[8,2048]{1,0:T(8,128)(2,1)S(1)}, bf16[8,2048]{1,0:T(8,128)(2,1)S(1)}, u32[]{:S(2)}, u32[]{:S(2)}) collective-permute-start(bf16[8,2048]{1,0:T(8,128)(2,1)S(1)} %pad_maximum_fusion.1), channel_id=1, source_target_pairs={{2,0},{4,2},{6,4},{8,6},{10,8},{12,10},{14,12},{16,14},{18,16},{20... | collective-permute-start | bytes 98312 | tf_op jit(solution)/shard_map/ppermute | solution.py:31
  26.8 201.4 %all-gather.5.cloned.1.call-start = ((), (), s32[]{:S(2)}) async-start(), calls=%async_computation.1 | async-start | bytes 5242880 | tf_op jit(solution)/shard_map/all_gather | solution.py:633
  26.9 55.4 %collective-permute-start.16 = (f32[1,1024]{1,0:T(1,128)S(1)}, f32[1,1024]{1,0:T(1,128)S(1)}, u32[]{:S(2)}, u32[]{:S(2)}) collective-permute-start(f32[1,1024]{1,0:T(1,128)S(1)} %bitcast.61), channel_id=1, source_target_pairs={{0,1},{1,0},{2,3},{3,2},{4,5},{5,4},{6,7},{7,6},{8,9},{9,8},{10,11... | collective-permute-start | bytes 12296 | tf_op jit(solution)/shard_map/ppermute | solution.py:46
  26.9 96.5 %collective-permute-start.15 = (bf16[768,1024]{1,0:T(8,128)(2,1)}, bf16[768,1024]{1,0:T(8,128)(2,1)}, u32[]{:S(2)}, u32[]{:S(2)}) collective-permute-start(bf16[768,1024]{1,0:T(8,128)(2,1)} %param.33), channel_id=1, source_target_pairs={{0,1},{1,0},{2,3},{3,2},{4,5},{5,4},{6,7},{7,6},{8,9},{9,8},{10,11... | collective-permute-start | bytes 4718600 | tf_op jit(solution)/shard_map/ppermute | solution.py:46
  35.5 69.1 %collective-permute-start.22 = (bf16[128,1024]{1,0:T(8,128)(2,1)}, bf16[128,1024]{1,0:T(8,128)(2,1)}, u32[]{:S(2)}, u32[]{:S(2)}) collective-permute-start(bf16[128,1024]{1,0:T(8,128)(2,1)} %get-tuple-element.72), channel_id=1, source_target_pairs={{0,2},{2,0},{4,6},{6,4},{1,3},{3,1},{5,7},{7,5},{8,10},{10,8},{12,... | collective-permute-start | bytes 786440 | tf_op jit(solution)/shard_map/ppermute | solution.py:39
  80.0 8.9 %collective-permute-start.7 = (bf16[2,4,48,256]{3,2,1,0:T(8,128)(2,1)}, bf16[2,4,48,256]{3,2,1,0:T(8,128)(2,1)S(1)}, u32[]{:S(2)}, u32[]{:S(2)}) collective-permute-start(bf16[2,4,48,256]{3,2,1,0:T(8,128)(2,1)} %get-tuple-element.77), channel_id=1, source_target_pairs={{0,6},{2,4},{4,2},{6,0},{1,7},{3,5},{5,3},{7,1},{8,14},{10,12},{12... | collective-permute-start | bytes 589832 | tf_op jit(solution)/shard_map/ppermute | solution.py:39
  81.1 12.2 %collective-permute-start.6 = (bf16[2,4,48,256]{3,2,1,0:T(8,128)(2,1)}, bf16[2,4,48,256]{3,2,1,0:T(8,128)(2,1)S(1)}, u32[]{:S(2)}, u32[]{:S(2)}) collective-permute-start(bf16[2,4,48,256]{3,2,1,0:T(8,128)(2,1)} %get-tuple-element.78), channel_id=1, source_target_pairs={{0,4},{2,6},{4,0},{6,2},{1,5},{3,7},{5,1},{7,3},{8,12},{10,14},{12... | collective-permute-start | bytes 589832 | tf_op jit(solution)/shard_map/ppermute | solution.py:39
  82.2 11.0 %collective-permute-start.5 = (bf16[2,4,48,256]{3,2,1,0:T(8,128)(2,1)}, bf16[2,4,48,256]{3,2,1,0:T(8,128)(2,1)}, u32[]{:S(2)}, u32[]{:S(2)}) collective-permute-start(bf16[2,4,48,256]{3,2,1,0:T(8,128)(2,1)} %get-tuple-element.79), channel_id=1, source_target_pairs={{0,2},{2,0},{4,6},{6,4},{1,3},{3,1},{5,7},{7,5},{8,10},{10,8},{12,... | collective-permute-start | bytes 589832 | tf_op jit(solution)/shard_map/ppermute | solution.py:39
  83.6 41.5 %copy-start.23 = (f32[1,2048]{1,0:T(1,128)}, f32[1,2048]{1,0:T(1,128)S(1)}, u32[]{:S(2)}) copy-start(f32[1,2048]{1,0:T(1,128)S(1)} %constant_dynamic-update-slice_fusion.refs_3_) | copy-start | bytes 24580
  88.9 18.6 %collective-permute-start.23 = (bf16[128,1024]{1,0:T(8,128)(2,1)}, bf16[128,1024]{1,0:T(8,128)(2,1)}, u32[]{:S(2)}, u32[]{:S(2)}) collective-permute-start(bf16[128,1024]{1,0:T(8,128)(2,1)} %get-tuple-element.71), channel_id=1, source_target_pairs={{0,4},{2,6},{4,0},{6,2},{1,5},{3,7},{5,1},{7,3},{8,12},{10,14},{12... | collective-permute-start | bytes 786440 | tf_op jit(solution)/shard_map/ppermute | solution.py:39
  97.1 13.7 %collective-permute-start.9 = (bf16[4,48,256]{2,1,0:T(8,128)(2,1)}, bf16[4,48,256]{2,1,0:T(8,128)(2,1)S(1)}, u32[]{:S(2)}, u32[]{:S(2)}) collective-permute-start(bf16[4,48,256]{2,1,0:T(8,128)(2,1)} %get-tuple-element.38), channel_id=1, source_target_pairs={{0,16},{8,24},{1,17},{9,25},{2,18},{10,26},{3,19},{11,27},{4,20},{... | collective-permute-start | bytes 294920 | tf_op jit(solution)/shard_map/ppermute | solution.py:31
  101.5 11.0 %collective-permute-start.8 = (bf16[4,48,256]{2,1,0:T(8,128)(2,1)}, bf16[4,48,256]{2,1,0:T(8,128)(2,1)}, u32[]{:S(2)}, u32[]{:S(2)}) collective-permute-start(bf16[4,48,256]{2,1,0:T(8,128)(2,1)} %get-tuple-element.38), channel_id=1, source_target_pairs={{0,8},{8,16},{16,24},{1,9},{9,17},{17,25},{2,10},{10,18},{18,26},{... | collective-permute-start | bytes 294920 | tf_op jit(solution)/shard_map/ppermute | solution.py:31
  104.6 8.3 %collective-permute-start.11 = (bf16[4,48,256]{2,1,0:T(8,128)(2,1)}, bf16[4,48,256]{2,1,0:T(8,128)(2,1)}, u32[]{:S(2)}, u32[]{:S(2)}) collective-permute-start(bf16[4,48,256]{2,1,0:T(8,128)(2,1)} %get-tuple-element.39), channel_id=1, source_target_pairs={{16,0},{24,8},{17,1},{25,9},{18,2},{26,10},{19,3},{27,11},{20,4},{... | collective-permute-start | bytes 294920 | tf_op jit(solution)/shard_map/ppermute | solution.py:31
  107.6 7.3 %collective-permute-start.10 = (bf16[4,48,256]{2,1,0:T(8,128)(2,1)}, bf16[4,48,256]{2,1,0:T(8,128)(2,1)}, u32[]{:S(2)}, u32[]{:S(2)}) collective-permute-start(bf16[4,48,256]{2,1,0:T(8,128)(2,1)} %get-tuple-element.39), channel_id=1, source_target_pairs={{8,0},{16,8},{24,16},{9,1},{17,9},{25,17},{10,2},{18,10},{26,18},{... | collective-permute-start | bytes 294920 | tf_op jit(solution)/shard_map/ppermute | solution.py:31
  110.7 36.0 %collective-permute-start.24 = (bf16[128,1024]{1,0:T(8,128)(2,1)}, bf16[128,1024]{1,0:T(8,128)(2,1)S(1)}, u32[]{:S(2)}, u32[]{:S(2)}) collective-permute-start(bf16[128,1024]{1,0:T(8,128)(2,1)} %get-tuple-element.70), channel_id=1, source_target_pairs={{0,6},{2,4},{4,2},{6,0},{1,7},{3,5},{5,3},{7,1},{8,14},{10,12},{12... | collective-permute-start | bytes 786440 | tf_op jit(solution)/shard_map/ppermute | solution.py:39
  119.9 7.2 %collective-permute-start.14 = (bf16[4,32,512]{2,1,0:T(8,128)(2,1)S(1)}, bf16[4,32,512]{2,1,0:T(8,128)(2,1)S(1)}, u32[]{:S(2)}, u32[]{:S(2)}) collective-permute-start(bf16[4,32,512]{2,1,0:T(8,128)(2,1)S(1)} %get-tuple-element.85), channel_id=1, source_target_pairs={{0,6},{2,4},{4,2},{6,0},{1,7},{3,5},{5,3},{7,1},{8,14},{10,12},{12... | collective-permute-start | bytes 393224 | tf_op jit(solution)/shard_map/ppermute | solution.py:39
  121.6 7.1 %collective-permute-start.13 = (bf16[4,32,512]{2,1,0:T(8,128)(2,1)S(1)}, bf16[4,32,512]{2,1,0:T(8,128)(2,1)}, u32[]{:S(2)}, u32[]{:S(2)}) collective-permute-start(bf16[4,32,512]{2,1,0:T(8,128)(2,1)S(1)} %get-tuple-element.86), channel_id=1, source_target_pairs={{0,4},{2,6},{4,0},{6,2},{1,5},{3,7},{5,1},{7,3},{8,12},{10,14},{12... | collective-permute-start | bytes 393224 | tf_op jit(solution)/shard_map/ppermute | solution.py:39
  122.1 6.6 %collective-permute-start.12 = (bf16[4,32,512]{2,1,0:T(8,128)(2,1)S(1)}, bf16[4,32,512]{2,1,0:T(8,128)(2,1)}, u32[]{:S(2)}, u32[]{:S(2)}) collective-permute-start(bf16[4,32,512]{2,1,0:T(8,128)(2,1)S(1)} %get-tuple-element.87), channel_id=1, source_target_pairs={{0,2},{2,0},{4,6},{6,4},{1,3},{3,1},{5,7},{7,5},{8,10},{10,8},{12,... | collective-permute-start | bytes 393224 | tf_op jit(solution)/shard_map/ppermute | solution.py:39
  146.7 5.9 %collective-permute-start.17 = (bf16[768,2048]{1,0:T(8,128)(2,1)}, bf16[768,2048]{1,0:T(8,128)(2,1)S(1)}, u32[]{:S(2)}, u32[]{:S(2)}) collective-permute-start(bf16[768,2048]{1,0:T(8,128)(2,1)} %convolution_convert_fusion.refs_0_), channel_id=1, source_target_pairs={{0,1},{1,0},{2,3},{3,2},{4,5},{5,4},{6,7},{7,6},{8,9},{9,8},{10,11... | collective-permute-start | bytes 9437192 | tf_op jit(solution)/shard_map/ppermute | solution.py:46
  162.7 36.6 %collective-permute-start.19 = (bf16[768,1024]{1,0:T(8,128)(2,1)}, bf16[768,1024]{1,0:T(8,128)(2,1)S(1)}, u32[]{:S(2)}, u32[]{:S(2)}) collective-permute-start(bf16[768,1024]{1,0:T(8,128)(2,1)} %get-tuple-element.46.own_ref), channel_id=1, source_target_pairs={{0,4},{2,6},{4,0},{6,2},{1,5},{3,7},{5,1},{7,3},{8,12},{10,14},{12... | collective-permute-start | bytes 4718600 | tf_op jit(solution)/shard_map/ppermute | solution.py:39
  163.2 36.4 %collective-permute-start.18 = (bf16[768,1024]{1,0:T(8,128)(2,1)}, bf16[768,1024]{1,0:T(8,128)(2,1)S(1)}, u32[]{:S(2)}, u32[]{:S(2)}) collective-permute-start(bf16[768,1024]{1,0:T(8,128)(2,1)} %get-tuple-element.46.own_ref), channel_id=1, source_target_pairs={{0,2},{2,0},{4,6},{6,4},{1,3},{3,1},{5,7},{7,5},{8,10},{10,8},{12,... | collective-permute-start | bytes 4718600 | tf_op jit(solution)/shard_map/ppermute | solution.py:39
  199.6 3.5 collective-permute-start.20
  199.6 10.8 %collective-permute-start.21 = (bf16[768,1024]{1,0:T(8,128)(2,1)S(1)}, bf16[768,1024]{1,0:T(8,128)(2,1)}, u32[]{:S(2)}, u32[]{:S(2)}) collective-permute-start(bf16[768,1024]{1,0:T(8,128)(2,1)S(1)} %collective-permute-done.19.own_ref), channel_id=1, source_target_pairs={{0,1},{1,0},{2,3},{3,2},{4,5},{5,4},{6,7},{7,6},{8,9},{9,8},{10,11... | collective-permute-start | bytes 4718600 | tf_op jit(solution)/shard_map/ppermute | solution.py:46
  246.3 8.0 %collective-permute-start.25 = (bf16[2304,1024]{1,0:T(8,128)(2,1)S(1)}, bf16[2304,1024]{1,0:T(8,128)(2,1)S(1)}, u32[]{:S(2)}, u32[]{:S(2)}) collective-permute-start(bf16[2304,1024]{1,0:T(8,128)(2,1)S(1)} %slice_bitcast_fusion), channel_id=1, source_target_pairs={{0,1},{1,0},{2,3},{3,2},{4,5},{5,4},{6,7},{7,6},{8,9},{9,8},{10,11... | collective-permute-start | bytes 14155784 | tf_op jit(solution)/shard_map/ppermute | solution.py:672
  246.5 20.0 %collective-permute-start.27 = (bf16[384,1024]{1,0:T(8,128)(2,1)S(1)}, bf16[384,1024]{1,0:T(8,128)(2,1)S(1)}, u32[]{:S(2)}, u32[]{:S(2)}) collective-permute-start(bf16[384,1024]{1,0:T(8,128)(2,1)S(1)} %slice.86), channel_id=1, source_target_pairs={{0,2},{2,0},{4,6},{6,4},{1,3},{3,1},{5,7},{7,5},{8,10},{10,8},{12,... | collective-permute-start | bytes 2359304 | tf_op jit(solution)/shard_map/ppermute | solution.py:39
  248.0 19.7 %collective-permute-start.26 = (bf16[384,1024]{1,0:T(8,128)(2,1)S(1)}, bf16[384,1024]{1,0:T(8,128)(2,1)S(1)}, u32[]{:S(2)}, u32[]{:S(2)}) collective-permute-start(bf16[384,1024]{1,0:T(8,128)(2,1)S(1)} %slice.85), channel_id=1, source_target_pairs={{0,4},{2,6},{4,0},{6,2},{1,5},{3,7},{5,1},{7,3},{8,12},{10,14},{12... | collective-permute-start | bytes 2359304 | tf_op jit(solution)/shard_map/ppermute | solution.py:39
  267.7 2.3 collective-permute-start.30
  267.7 8.1 %collective-permute-start.31 = (bf16[384,1024]{1,0:T(8,128)(2,1)S(1)}, bf16[384,1024]{1,0:T(8,128)(2,1)S(1)}, u32[]{:S(2)}, u32[]{:S(2)}) collective-permute-start(bf16[384,1024]{1,0:T(8,128)(2,1)S(1)} %collective-permute-done.27.own_ref), channel_id=1, source_target_pairs={{0,1},{1,0},{2,3},{3,2},{4,5},{5,4},{6,7},{7,6},{8,9},{9,8},{10,11... | collective-permute-start | bytes 2359304 | tf_op jit(solution)/shard_map/ppermute | solution.py:46
  290.4 4.6 %collective-permute-start.32 = (bf16[768,1024]{1,0:T(8,128)(2,1)S(1)}, bf16[768,1024]{1,0:T(8,128)(2,1)S(1)}, u32[]{:S(2)}, u32[]{:S(2)}) collective-permute-start(bf16[768,1024]{1,0:T(8,128)(2,1)S(1)} %slice_bitcast_fusion.2), channel_id=1, source_target_pairs={{0,1},{1,0},{2,3},{3,2},{4,5},{5,4},{6,7},{7,6},{8,9},{9,8},{10,11... | collective-permute-start | bytes 4718600 | tf_op jit(solution)/shard_map/ppermute | solution.py:672
  293.0 56.9 %collective-permute-start.28 = (bf16[768,1024]{1,0:T(8,128)(2,1)S(1)}, bf16[768,1024]{1,0:T(8,128)(2,1)S(1)}, u32[]{:S(2)}, u32[]{:S(2)}) collective-permute-start(bf16[768,1024]{1,0:T(8,128)(2,1)S(1)} %get-tuple-element.64), channel_id=1, source_target_pairs={{0,2},{2,0},{4,6},{6,4},{1,3},{3,1},{5,7},{7,5},{8,10},{10,8},{12,... | collective-permute-start | bytes 4718600 | tf_op jit(solution)/shard_map/ppermute | solution.py:39
  293.6 73.3 %copy-start.3 = (bf16[768,1024]{1,0:T(8,128)(2,1)S(1)}, bf16[768,1024]{1,0:T(8,128)(2,1)}, u32[]{:S(2)}) copy-start(bf16[768,1024]{1,0:T(8,128)(2,1)} %get-tuple-element.46.own_ref) | copy-start | bytes 4718596
  293.6 56.3 %collective-permute-start.29 = (bf16[768,1024]{1,0:T(8,128)(2,1)S(1)}, bf16[768,1024]{1,0:T(8,128)(2,1)S(1)}, u32[]{:S(2)}, u32[]{:S(2)}) collective-permute-start(bf16[768,1024]{1,0:T(8,128)(2,1)S(1)} %get-tuple-element.65), channel_id=1, source_target_pairs={{0,4},{2,6},{4,0},{6,2},{1,5},{3,7},{5,1},{7,3},{8,12},{10,14},{12... | collective-permute-start | bytes 4718600 | tf_op jit(solution)/shard_map/ppermute | solution.py:39
  295.9 51.0 %collective-permute-start.33 = (bf16[384,1024]{1,0:T(8,128)(2,1)S(1)}, bf16[384,1024]{1,0:T(8,128)(2,1)S(1)}, u32[]{:S(2)}, u32[]{:S(2)}) collective-permute-start(bf16[384,1024]{1,0:T(8,128)(2,1)S(1)} %get-tuple-element.66), channel_id=1, source_target_pairs={{0,4},{2,6},{4,0},{6,2},{1,5},{3,7},{5,1},{7,3},{8,12},{10,14},{12... | collective-permute-start | bytes 2359304 | tf_op jit(solution)/shard_map/ppermute | solution.py:39
  296.5 74.5 %copy-start.26 = (f32[1024]{0:T(1024)S(1)}, f32[1024]{0:T(1024)}, u32[]{:S(2)}) copy-start(f32[1024]{0:T(1024)} %param.35) | copy-start | bytes 12292
  296.5 51.9 %collective-permute-start.35 = (bf16[384,1024]{1,0:T(8,128)(2,1)S(1)}, bf16[384,1024]{1,0:T(8,128)(2,1)S(1)}, u32[]{:S(2)}, u32[]{:S(2)}) collective-permute-start(bf16[384,1024]{1,0:T(8,128)(2,1)S(1)} %get-tuple-element.67), channel_id=1, source_target_pairs={{0,2},{2,0},{4,6},{6,4},{1,3},{3,1},{5,7},{7,5},{8,10},{10,8},{12,... | collective-permute-start | bytes 2359304 | tf_op jit(solution)/shard_map/ppermute | solution.py:39
  346.9 18.8 %collective-permute-start.34 = (bf16[384,1024]{1,0:T(8,128)(2,1)S(1)}, bf16[384,1024]{1,0:T(8,128)(2,1)S(1)}, u32[]{:S(2)}, u32[]{:S(2)}) collective-permute-start(bf16[384,1024]{1,0:T(8,128)(2,1)S(1)} %collective-permute-done.33), channel_id=1, source_target_pairs={{0,2},{2,0},{4,6},{6,4},{1,3},{3,1},{5,7},{7,5},{8,10},{10,8},{12,... | collective-permute-start | bytes 2359304 | tf_op jit(solution)/shard_map/ppermute | solution.py:39
  348.4 18.5 %collective-permute-start.36 = (bf16[384,1024]{1,0:T(8,128)(2,1)S(1)}, bf16[384,1024]{1,0:T(8,128)(2,1)S(1)}, u32[]{:S(2)}, u32[]{:S(2)}) collective-permute-start(bf16[384,1024]{1,0:T(8,128)(2,1)S(1)} %collective-permute-done.35), channel_id=1, source_target_pairs={{0,4},{2,6},{4,0},{6,2},{1,5},{3,7},{5,1},{7,3},{8,12},{10,14},{12... | collective-permute-start | bytes 2359304 | tf_op jit(solution)/shard_map/ppermute | solution.py:39
  369.8 1.2 collective-permute-start.37
  (21 other events, 130.6 us)
Sparse Core Ops, SparseCore 0:
  26.9 80.9 all-gather.2
  147.6 80.5 all-gather.4
where the time goes:
time: 381 us; the launch traced here: 379 us
  waiting for transfers between devices  146 us (38%)
  Pallas kernels  120 us (31%)
  starting transfers between devices  45.8 us (12%)
  local copies, waits for them, and re-layouts  35.7 us (9%)
  between operations  13.9 us (4%)
  other arithmetic  9.95 us (3%)
  matrix products  7.72 us (2%)
    ppermute x22, waiting for transfers between devices, partner(): lax.ppermute(array, 'inner', [(i, i ^ turn) for i in range(lax.axis_size(...  111 us
    pallas_call x1, Pallas kernels, mixer(): pl.pallas_call(functools.partial(mixer_kernel, first_group=first), grid=(...  41 us
    pallas_call x5, Pallas kernels, up_rows(): pl.pallas_call(up_kernel, grid=(units // tile,), in_specs=[pl.BlockSpec(m...  31.6 us
    ppermute x22, starting transfers between devices, partner(): lax.ppermute(array, 'inner', [(i, i ^ turn) for i in range(lax.axis_size(...  28.5 us
    pallas_call x2, Pallas kernels, down_rows(): pl.pallas_call(down_kernel, grid_spec=grid_spec, out_shape=jax.ShapeDtype...  22.4 us
    ppermute x6, starting transfers between devices, shifted(): return lax.ppermute(array, axis, pairs)  15.3 us
    all_gather x1, waiting for transfers between devices, per_device(): down_weights = lax.all_gather(swap_finish(down_swaps), 'outer')  10.6 us
    pallas_call x1, Pallas kernels, per_device(): pl.pallas_call(gate_kernel, grid=(groups,), in_specs=[smem, rows_spec(wid...  10.3 us
  transfers between devices with their start and end apart: 40, of which 20 were waited for; matrix products, arithmetic and copies ran while one was open for 10% of the time, Pallas kernels for 24%

commit v1 on v0

--- a/solution.py
+++ b/solution.py
@@ -89,15 +89,6 @@
     return pieces
 
 
-def swap_finish(pieces):
-    place = lax.axis_index("inner")
-    rows, width = pieces[0].shape
-    joined = jnp.zeros((rows * len(pieces), width), pieces[0].dtype)
-    for turn, piece in enumerate(pieces):
-        joined = lax.dynamic_update_slice_in_dim(joined, piece, (place ^ turn) * rows, axis=0)
-    return joined
-
-
 def sum_tp(pair):
     if lax.axis_size("tp") == 2:
         return pair + lax.ppermute(pair, "tp", [(0, 1), (1, 0)])
@@ -133,7 +124,7 @@
     first_group,
 ):
     (out_ref, readout_out_ref, far_ref, end_ref,
-     window, values, entries, fresh, starts, cols, lines, sums) = rest[-12:]
+     window, values, entries, fresh, starts, cols, lines) = rest[-11:]
     rows, width = value_ref.shape
     per = width // HEAD_DIM
     both = 2 * per
@@ -151,15 +142,78 @@
         window[edge : edge + rows, to : to + 128] = source[:, at : at + 128].astype(f32)
 
     heads = step_ref.shape[1]
-    head = lax.broadcasted_iota(jnp.int32, (heads, both), 0)
-    lane = lax.broadcasted_iota(jnp.int32, (heads, both), 1)
-    pick = head == (first_group + pl.program_id(0)) * per + jnp.where(lane < per, lane, lane - per)
-    pick = jnp.where(pick, 1.0, 0.0)
+    wide = blocks * both
+    first_head = (first_group + pl.program_id(0)) * per
+    head = lax.broadcasted_iota(jnp.int32, (heads, wide), 0)
+    lane = lax.broadcasted_iota(jnp.int32, (heads, wide), 1)
     at = lax.broadcasted_iota(jnp.int32, (BLOCK, BLOCK), 0)
     source_at = lax.broadcasted_iota(jnp.int32, (BLOCK, BLOCK), 1)
     lower = jnp.where(at >= source_at, 1.0, 0.0)
     unit = jnp.where(at == source_at, 1.0, 0.0)
-    ahead_lane = lax.broadcasted_iota(jnp.int32, (1, both), 1) < per
+    block_lane = lax.broadcasted_iota(jnp.int32, (1, wide), 1)
+    ahead_lane = block_lane % both < per
+    raw = jnp.zeros((BLOCK, wide), f32)
+    sudden = jnp.zeros((BLOCK, wide), f32)
+    own = jnp.zeros((BLOCK, wide), f32)
+    before = jnp.zeros((1, wide), f32)
+    after = jnp.zeros((1, wide), f32)
+    for b in range(blocks):
+        here = slice(b * BLOCK, (b + 1) * BLOCK)
+        pick = (lane // both == b) & (head == first_head + lane % per)
+        pick = jnp.where(pick, 1.0, 0.0)
+        raw = raw + jnp.dot(step_ref[here, :], pick.astype(bf16), preferred_element_type=f32)
+        sudden = sudden + jnp.dot(
+            sudden_ref[here, :], pick, precision=exact_prec, preferred_element_type=f32
+        )
+        mine = block_lane // both == b
+        top = edge + b * BLOCK
+        own = jnp.where(mine, doc_ref[top : top + BLOCK, :], own)
+        before = jnp.where(mine, doc_ref[top - 1 : top, :], before)
+        after = jnp.where(mine, doc_ref[top + BLOCK : top + BLOCK + 1, :], after)
+
+    def along_lanes(ref):
+        every = jnp.where(head == first_head + lane % per, 1.0, 0.0)
+        both_ways = jnp.dot(ref[...], every, precision=exact_prec, preferred_element_type=f32)
+        return jnp.where(ahead_lane, both_ways[0:1], both_ways[1:2])
+
+    raw = raw + along_lanes(bias_ref)
+    step = jnp.maximum(raw, 0.0) + jnp.log1p(jnp.exp(-jnp.abs(raw)))
+    decay = (sudden - jnp.exp(along_lanes(rate_ref)) * step) * LOG2E
+    cum = jnp.dot(lower, decay, precision=exact_prec, preferred_element_type=f32)
+    total = cum[BLOCK - 1 : BLOCK]
+    cum = jnp.where(ahead_lane, cum, total - cum + decay)
+    leave = jnp.where(ahead_lane, own[BLOCK - 1 : BLOCK], own[0:1])
+    come = jnp.where(ahead_lane, before, after)
+    outward = jnp.where(own == leave, jnp.exp2(total - cum) * step, 0.0)
+    arrive = jnp.where(own == come, jnp.exp2(cum), 0.0)
+    passing = jnp.where(leave == come, jnp.exp2(total), 0.0)
+    row = lax.broadcasted_iota(jnp.int32, (wide, wide), 0)
+    col = lax.broadcasted_iota(jnp.int32, (wide, wide), 1)
+    forward_col = col % both < per
+    nearer = (forward_col & (row < col)) | ((col % both >= per) & (row > col))
+    between = jnp.where((row % both == col % both) & nearer, 1.0, 0.0)
+    offset = jnp.dot(
+        jnp.broadcast_to(total, (8, wide)), between, precision=exact_prec, preferred_element_type=f32
+    )[0:1]
+    turned = (row // both == col // both) & (row % per == col % per) & (row != col)
+    other_step = jnp.dot(
+        step, jnp.where(turned, 1.0, 0.0), precision=exact_prec, preferred_element_type=f32
+    )
+    prev_doc = doc_ref[edge - 1 : edge, :]
+    next_doc = doc_ref[edge + rows : edge + rows + 1, :]
+    beyond = jnp.where(ahead_lane, prev_doc, next_doc)
+    far = jnp.where(own == beyond, jnp.exp2(cum + offset), 0.0)
+    whole = jnp.where(beyond == leave, jnp.exp2(total + offset), 0.0)
+    for k, part in enumerate((jnp.log2(step) - cum, jnp.log2(step + other_step))):
+        lines[k * wide : (k + 1) * wide] = lax.dot_general(
+            part, unit, (((0,), (0,)), ((), ())), precision=exact_prec, preferred_element_type=f32
+        )
+    for b in range(blocks):
+        span = slice(b * both, (b + 1) * both)
+        cols[b, :, 0:both] = cum[:, span]
+        cols[b, :, both : 2 * both] = arrive[:, span]
+        cols[b, :, 2 * both : 3 * both] = outward[:, span]
+        far_ref[b * BLOCK : (b + 1) * BLOCK, :] = far[:, span]
 
     def conv_block(b, _):
         start = pl.multiple_of(b * BLOCK, BLOCK)
@@ -170,28 +224,7 @@
             jnp.where(docs[edge - half + k : edge - half + k + BLOCK] == own, 1.0, 0.0)
             for k in range(taps)
         ]
-        raw = jnp.dot(step_ref[here, :].astype(f32), pick, preferred_element_type=f32)
-        sudden = jnp.dot(sudden_ref[here, :], pick, precision=exact_prec, preferred_element_type=f32)
-        raw = raw + bias_ref[...]
-        step = jnp.maximum(raw, 0.0) + jnp.log1p(jnp.exp(-jnp.abs(raw)))
-        decay = (sudden - jnp.exp(rate_ref[...]) * step) * LOG2E
-        cum = jnp.dot(lower, decay, precision=exact_prec, preferred_element_type=f32)
-        total = cum[BLOCK - 1 : BLOCK]
-        cum = jnp.where(ahead_lane, cum, total - cum + decay)
-        leave = jnp.where(ahead_lane, own[BLOCK - 1 : BLOCK], own[0:1])
-        come = jnp.where(ahead_lane, docs[edge - 1 : edge], docs[edge + BLOCK : edge + BLOCK + 1])
-        outward = jnp.where(own == leave, jnp.exp2(total - cum) * step, 0.0)
-        arrive = jnp.where(own == come, jnp.exp2(cum), 0.0)
-        passing = jnp.where(leave == come, jnp.exp2(total), 0.0)
-        single = jnp.log2(step[:, :per] + step[:, per:])
-        cols[here, 0:both] = cum
-        cols[here, both : 2 * both] = arrive
-        line = jnp.concatenate([jnp.log2(step) - cum, single, single], axis=1)
-        lines[b] = lax.dot_general(
-            line, unit, (((0,), (0,)), ((), ())), precision=exact_prec, preferred_element_type=f32
-        )
-        sums[b, 0:1, 0:both] = total
-        sums[b, 1:2, 0:both] = passing
+        outward = cols[b, :, 2 * both : 3 * both]
         value_parts = []
         for source, low, high, tap_ref, at, to in pieces:
             around = window[pl.ds(start, BLOCK + 2 * edge), to : to + 128]
@@ -220,35 +253,21 @@
         )
         return 0
 
-    lax.fori_loop(0, blocks, conv_block, 0)
-
-    prev_doc = doc_ref[edge - 1 : edge, :]
-    next_doc = doc_ref[edge + rows : edge + rows + 1, :]
-    first_doc = doc_ref[edge : edge + 1, :]
-    last_doc = doc_ref[edge + rows - 1 : edge + rows, :]
-    totals = [sums[b, 0:1, 0:both] for b in range(blocks)]
-    passes = [sums[b, 1:2, 0:both] for b in range(blocks)]
-    for b in range(blocks):
-        nothing = jnp.zeros((1, both), f32)
-        sums[b, 2:3, 0:both] = jnp.where(
-            ahead_lane, sum(totals[:b], nothing), sum(totals[b + 1 :], nothing)
-        )
-    whole = jnp.where(
-        jnp.where(ahead_lane, prev_doc, next_doc) == jnp.where(ahead_lane, last_doc, first_doc),
-        jnp.exp2(sum(totals[1:], totals[0])), 0.0,
-    )
+    lax.fori_loop(0, blocks, conv_block, 0, unroll=2)
+
     tail_row = lax.broadcasted_iota(jnp.int32, (16, width), 0)
     for k, order in ((0, range(blocks)), (1, range(blocks - 1, -1, -1))):
         span = slice(k * width, (k + 1) * width)
         state = jnp.zeros((STATE, width), f32)
         for b in order:
             starts[b, :, span] = state.astype(bf16)
-            factor = spread(passes[b][:, k * per : (k + 1) * per], per)
+            factor = spread(passing[:, b * both + k * per : b * both + (k + 1) * per], per)
             state = state * factor + fresh[b, :, span]
         share = STATE // SIDE
         for q in range(SIDE):
             end_ref[q, k, 0:share] = state[q * share : (q + 1) * share].astype(bf16)
-        factor = spread(whole[:, k * per : (k + 1) * per], per)
+        edge_block = (blocks - 1, 0)[k] * both + k * per
+        factor = spread(whole[:, edge_block : edge_block + per], per)
         coarse = factor.astype(bf16).astype(f32)
         tail = jnp.where(tail_row == 0, coarse, jnp.where(tail_row == 1, factor - coarse, 0.0))
         for q in range(SIDE):
@@ -258,11 +277,10 @@
         start = pl.multiple_of(b * BLOCK, BLOCK)
         here = pl.ds(start, BLOCK)
         own = doc_ref[pl.ds(start + edge, BLOCK), :]
-        cum = cols[here, 0:both]
-        arrive = cols[here, both : 2 * both]
-        beyond = jnp.where(ahead_lane, prev_doc, next_doc)
-        far_ref[here, :] = jnp.where(own == beyond, jnp.exp2(cum + sums[b, 2:3, 0:both]), 0.0)
-        along = lines[b]
+        cum = cols[b, :, 0:both]
+        arrive = cols[b, :, both : 2 * both]
+        along = lines[pl.ds(pl.multiple_of(b * both, both), both), :]
+        singles = lines[pl.ds(pl.multiple_of(wide + b * both, both), both), :]
         readout = readout_out_ref[here, :]
         entry = entries[here, :]
         value = values[here, :]
@@ -278,7 +296,7 @@
         for r in range(per):
             ahead = cum[:, r : r + 1] + along[r : r + 1, :]
             behind = cum[:, per + r : per + r + 1] + along[per + r : per + r + 1, :]
-            single = along[both + r : both + r + 1, :]
+            single = singles[r : r + 1, :]
             power = jnp.where(at > source_at, ahead, jnp.where(at < source_at, behind, single))
             weights.append((scores * jnp.exp2(power)).astype(bf16))
             mine = (value_lane >= r * HEAD_DIM) & (value_lane < (r + 1) * HEAD_DIM)
@@ -294,7 +312,7 @@
         out_ref[here, :] = total
         return 0
 
-    lax.fori_loop(0, blocks, out_block, 0)
+    lax.fori_loop(0, blocks, out_block, 0, unroll=2)
 
 
 def opened(packed):
@@ -366,79 +384,123 @@
         out_ref[here, :] = (total * scale * gain_ref[...]).astype(bf16)
         return 0
 
-    lax.fori_loop(0, rows // BLOCK, one, 0)
-
-
-def up_kernel(place_ref, own_ref, other_ref, weight_ref, out_ref, rows_ref):
-    depth = own_ref.shape[1]
-    outer, wide, tile = weight_ref.shape
+    lax.fori_loop(0, rows // BLOCK, one, 0, unroll=3)
+
+
+def up_kernel(place_ref, inner_ref, *refs):
+    pieces, (weight_ref, out_ref, rows_ref) = refs[:-3], refs[-3:]
+    depth = pieces[0].shape[1]
+    outer, turns, wide, tile = weight_ref.shape
 
     @pl.when(pl.program_id(0) == 0)
     def _():
-        place = place_ref[0]
-        rows_ref[:, pl.ds(pl.multiple_of(place * depth, depth), depth)] = own_ref[...]
-        rows_ref[:, pl.ds(pl.multiple_of((1 - place) * depth, depth), depth)] = other_ref[...]
-
-    weight = weight_ref[...].reshape(outer * wide, tile)
+        top = 0
+        for own_ref, other_ref in zip(pieces[::2], pieces[1::2]):
+            rows = own_ref.shape[0]
+            for half, source in ((place_ref[0], own_ref), (1 - place_ref[0], other_ref)):
+                for block in range(depth // wide):
+                    group, turn = block // turns, block % turns
+                    at = (group * turns + (inner_ref[0] ^ turn)) * wide
+                    to = half * depth + block * wide
+                    rows_ref[top : top + rows, pl.ds(pl.multiple_of(to, 128), wide)] = source[
+                        :, pl.ds(pl.multiple_of(at, 128), wide)
+                    ]
+            top += rows
+
+    weight = weight_ref[...].reshape(outer * turns * wide, tile)
     hidden = jnp.dot(rows_ref[...], weight, preferred_element_type=f32)
     hidden = jnp.maximum(hidden, 0.0)
     out_ref[...] = (hidden * hidden).astype(bf16)
 
 
-def up_rows(place, own, other, weights):
-    rows, depth = own.shape
-    outer, wide, units = weights.shape
-    tile = units // 2
+def up_rows(place, inner_place, pieces, weights):
+    depth = pieces[0].shape[1]
+    rows = sum(piece.shape[0] for piece in pieces[::2])
+    outer, turns, wide, units = weights.shape
+    tile = units // 4
+    smem = pl.BlockSpec(memory_space=pltpu.SMEM)
     return pl.pallas_call(
         up_kernel,
         grid=(units // tile,),
-        in_specs=[
-            pl.BlockSpec(memory_space=pltpu.SMEM),
-            pl.BlockSpec((rows, depth), lambda i: (0, 0)),
-            pl.BlockSpec((rows, depth), lambda i: (0, 0)),
-            pl.BlockSpec((outer, wide, tile), lambda i: (0, 0, i)),
+        in_specs=[smem, smem] + [pl.BlockSpec(p.shape, lambda i: (0, 0)) for p in pieces] + [
+            pl.BlockSpec((outer, turns, wide, tile), lambda i: (0, 0, 0, i)),
         ],
         out_specs=pl.BlockSpec((rows, tile), lambda i: (0, i)),
         out_shape=jax.ShapeDtypeStruct((rows, units), bf16),
         scratch_shapes=[pltpu.VMEM((rows, 2 * depth), bf16)],
         name="up_rows",
-    )(place, own, other, weights)
-
-
-def down_kernel(place_ref, *refs):
+    )(place, inner_place, *pieces, weights)
+
+
+def down_kernel(place_ref, inner_ref, *refs):
     pieces, (weight_ref, out_ref) = refs[:-2], refs[-2:]
+    turns, wide, units = weight_ref.shape
+    weight = weight_ref[...].reshape(turns * wide, units)
     at = 0
     for piece in pieces:
         rows = piece.shape[0]
-        out_ref[at : at + rows, :] = lax.dot_general(
-            piece[...], weight_ref[...], (((1,), (1,)), ((), ())), preferred_element_type=f32
+        product = lax.dot_general(
+            piece[...], weight, (((1,), (1,)), ((), ())), preferred_element_type=f32
         ).astype(bf16)
+        for turn in range(turns):
+            to = pl.multiple_of((inner_ref[0] ^ turn) * wide, 128)
+            out_ref[at : at + rows, pl.ds(to, wide)] = product[:, turn * wide : (turn + 1) * wide]
         at += rows
 
 
-def down_rows(place, pieces, weights):
+def down_rows(place, inner_place, pieces, weights):
     rows = sum(piece.shape[0] for piece in pieces)
-    outer, wide, units = weights.shape
+    outer, turns, wide, units = weights.shape
     half = outer // 2
     grid_spec = pltpu.PrefetchScalarGridSpec(
-        num_scalar_prefetch=1,
+        num_scalar_prefetch=2,
         grid=(outer,),
-        in_specs=[pl.BlockSpec(piece.shape, lambda i, place: (0, 0)) for piece in pieces] + [
+        in_specs=[pl.BlockSpec(piece.shape, lambda i, place, inner: (0, 0)) for piece in pieces] + [
             pl.BlockSpec(
-                (pl.Squeezed(), wide, units),
-                lambda i, place: ((i + place[0] * half) % outer, 0, 0),
+                (pl.Squeezed(), turns, wide, units),
+                lambda i, place, inner: ((i + place[0] * half) % outer, 0, 0, 0),
             )
         ],
         out_specs=pl.BlockSpec(
-            (pl.Squeezed(), rows, wide), lambda i, place: (i // half, 0, i % half)
+            (pl.Squeezed(), rows, turns * wide), lambda i, place, inner: (i // half, 0, i % half)
         ),
     )
     return pl.pallas_call(
         down_kernel,
         grid_spec=grid_spec,
-        out_shape=jax.ShapeDtypeStruct((2, rows, half * wide), bf16),
+        out_shape=jax.ShapeDtypeStruct((2, rows, half * turns * wide), bf16),
         name="down_rows",
-    )(place, *pieces, weights)
+    )(place, inner_place, *pieces, weights)
+
+
+def piece_kernel(here_ref, other_ref, *out_refs):
+    at = 0
+    for out_ref in out_refs:
+        span = slice(at, at + out_ref.shape[0])
+        out_ref[...] = (here_ref[span].astype(f32) + other_ref[span].astype(f32)).astype(bf16)
+        at += out_ref.shape[0]
+
+
+def summed_pieces(both, other, count):
+    rows, width = other.shape
+    shape = jax.ShapeDtypeStruct((rows // count, width), bf16)
+    return pl.pallas_call(
+        piece_kernel,
+        grid=(1,),
+        in_specs=[
+            pl.BlockSpec((pl.Squeezed(), rows, width), lambda i: (0, 0, 0)),
+            pl.BlockSpec((rows, width), lambda i: (0, 0)),
+        ],
+        out_specs=[pl.BlockSpec(shape.shape, lambda i: (0, 0))] * count,
+        out_shape=[shape] * count,
+        name="summed_pieces",
+    )(both, other)
+
+
+def in_order(weights):
+    place = lax.axis_index("inner")
+    turns = [lax.dynamic_index_in_dim(weights, place ^ j, 1, keepdims=True) for j in range(SIDE)]
+    return jnp.concatenate(turns, axis=1).reshape(-1, weights.shape[3])
 
 
 def norm_kernel(place_ref, *refs):
@@ -514,7 +576,7 @@
     high = shifted(joined_high, -1)
     up_swaps = swap_start(up_projection_weight)
     (low, high), up_swaps, down_own = together((low, high), up_swaps, down_projection_weight)
-    up_weights = lax.all_gather(swap_finish(up_swaps), "outer")
+    up_weights = lax.all_gather(jnp.stack(up_swaps), "outer")
     down_swaps = swap_start(down_own)
 
     position = lax.axis_index(SP) * row_count
@@ -522,9 +584,6 @@
     around = lax.dynamic_slice_in_dim(doc_pad, position, row_count + 2 * edge).astype(f32)
     doc_column = around[:, None]
     doc_rows = around[edge : edge + row_count].reshape(blocks, 1, BLOCK)
-
-    def lanes(array):
-        return array.reshape(2, groups, per).transpose(1, 0, 2).reshape(groups, 1, 2 * per)
 
     def rows_spec(columns_wide, first=0):
         return pl.BlockSpec((row_count, columns_wide), lambda g: (0, first + g))
@@ -553,7 +612,7 @@
         given = [
             head_value_rows, entry_map_rows, readout_map_rows, low, low, low, high, high, high,
             value_conv_taps, entry_conv_taps, readout_conv_taps, step_before_softplus,
-            sudden_log_decay, lanes(head_rate_logarithm), lanes(head_step_bias), doc_column, doc_rows,
+            sudden_log_decay, head_rate_logarithm, head_step_bias, doc_column, doc_rows,
         ]
         return pl.pallas_call(
             functools.partial(mixer_kernel, first_group=first),
@@ -564,7 +623,7 @@
                 thin_spec(taps, width, first), thin_spec(taps, STATE, first),
                 thin_spec(taps, STATE, first),
                 same_spec(row_count, head_count), same_spec(row_count, head_count),
-                group_spec(1, 2 * per, first=first), group_spec(1, 2 * per, first=first),
+                same_spec(2, head_count), same_spec(2, head_count),
                 same_spec(row_count + 2 * edge, 1), same_spec(blocks, 1, BLOCK),
             ] + [pl.BlockSpec(memory_space=pl.ANY)] * len(so_far),
             out_specs=[
@@ -587,9 +646,8 @@
                 pltpu.VMEM((row_count, STATE), bf16),
                 pltpu.VMEM((blocks, STATE, 2 * width), f32),
                 pltpu.VMEM((blocks, STATE, 2 * width), bf16),
-                pltpu.VMEM((row_count, 128), f32),
-                pltpu.VMEM((blocks, 4 * per, BLOCK), f32),
-                pltpu.VMEM((blocks, 8, 128), f32),
+                pltpu.VMEM((blocks, BLOCK, 128), f32),
+                pltpu.VMEM((4 * per * blocks, BLOCK), f32),
             ],
             name="mixer",
         )(*given, *so_far)
@@ -630,7 +688,7 @@
         name="arrive",
     )(inner_place, *shares, *others)
     packs = [arrivals[0]] + [partner(arrivals[turn], turn) for turn in (1, 2, 3)]
-    down_weights = lax.all_gather(swap_finish(down_swaps), "outer")
+    down_weights = lax.all_gather(jnp.stack(down_swaps), "outer")
 
     tp_count = lax.axis_size("tp")
     if tp_count == 2:
@@ -658,44 +716,52 @@
         own_one = norm_scattered(scattered(part), stream, mixer_norm_gain)
         other_one = None
 
-    def hidden_units(rows, other=None):
+    def hidden_units(pieces, others=None):
         if tp_count == 2:
-            other = over_tp(rows)[1] if other is None else other
-            return up_rows(place, rows, other, up_weights)
-        up = up_weights.reshape(-1, up_weights.shape[2])
-        hidden = jnp.dot(columns_over_tp(rows), up, preferred_element_type=f32)
+            others = [over_tp(rows)[1] for rows in pieces] if others is None else others
+            pairs = [array for pair in zip(pieces, others) for array in pair]
+            return up_rows(place, inner_place, pairs, up_weights)
+        up = in_order(up_weights)
+        rows = columns_over_tp(jnp.concatenate(pieces, axis=0))
+        hidden = jnp.dot(rows, up, preferred_element_type=f32)
         return jnp.square(jax.nn.relu(hidden)).astype(bf16)
 
-    def contributions(pieces):
+    def contributions(pieces, count=1):
         if tp_count == 2:
-            both = down_rows(place, pieces, down_weights)
+            both = down_rows(place, inner_place, pieces, down_weights)
             other = lax.ppermute(both[1], "tp", [(0, 1), (1, 0)])
+            if count > 1:
+                return summed_pieces(both, other, count)
             return (both[0].astype(f32) + other.astype(f32)).astype(bf16)
-        down = down_weights.reshape(-1, down_weights.shape[2])
+        down = in_order(down_weights)
         product = lax.dot_general(
             jnp.concatenate(pieces, axis=0), down, (((1,), (1,)), ((), ())),
             preferred_element_type=f32,
         )
-        return scattered(product.astype(bf16)).astype(bf16)
+        total = scattered(product.astype(bf16)).astype(bf16)
+        return jnp.split(total, count, axis=0) if count > 1 else total
 
     middle = row_count // 2
     side_one, side_two = partner(own_one, 1), partner(own_one, 2)
-    units = hidden_units(own_one, other_one)
+    units = hidden_units([own_one], [other_one])
     side_one, side_two, units = together(side_one, side_two, units)
     far_one = partner(side_one[:middle], 2)
     far_two = partner(side_two[middle:], 1)
-    near_units = [units, hidden_units(side_one), hidden_units(side_two)]
-    near = contributions(near_units)
-    far_rows = [far_one, far_two]
-    near, far_rows = together(near, far_rows)
-    back_one = partner(near[row_count : 2 * row_count], 1)
-    back_two = partner(near[2 * row_count :], 2)
-    diagonal_units = [hidden_units(rows) for rows in far_rows]
-    diagonal = contributions(diagonal_units)
-    first_hop = [partner(diagonal[:middle], 2), partner(diagonal[middle:], 1)]
-    second_hop = [partner(first_hop[0], 1), partner(first_hop[1], 2)]
-    added = near[:row_count].astype(f32) + back_one.astype(f32) + back_two.astype(f32)
-    added = added + jnp.concatenate(second_hop, axis=0).astype(f32)
+    near_units = hidden_units([side_one, side_two])
+    near_units, far_one, far_two = together(near_units, far_one, far_two)
+    late_one, ready_one, ready_two, late_two = contributions([near_units], 4)
+    early_one = partner(ready_one, 1)
+    early_two = partner(ready_two, 2)
+    diagonal_units = hidden_units([far_one, far_two])
+    for_hop_one, for_hop_two = contributions([diagonal_units], 2)
+    hop_one = partner(for_hop_one, 2)
+    hop_two = partner(for_hop_two, 1)
+    own_sum = contributions([units])
+    late_one = partner(late_one + hop_one, 1)
+    late_two = partner(late_two + hop_two, 2)
+    back_one = jnp.concatenate([late_one, early_one], axis=0).astype(f32)
+    back_two = jnp.concatenate([early_two, late_two], axis=0).astype(f32)
+    added = own_sum.astype(f32) + back_one + back_two
     return norm_scattered(added, own_one, channel_norm_gain)
 
 

time: 381 us -> 346 us (0.908)
  waiting for transfers between devices: 146 us -> 109 us
  local copies, waits for them, and re-layouts: 35.7 us -> 31 us
  starting transfers between devices: 45.8 us -> 50.4 us
    ppermute x22, waiting for transfers between devices: 111 us -> 86 us  [partner(): lax.ppermute(array, 'inner', [(i, i ^ turn) for i in range(lax.axis_size(...]
    pallas_call x1, Pallas kernels: 41 us -> 32.2 us  [mixer(): pl.pallas_call(functools.partial(mixer_kernel, first_group=first), grid=(...]
    pallas_call x5, Pallas kernels: 31.6 us -> 39.1 us  [the longest x3 31 us: up_rows(): pl.pallas_call(up_kernel, grid=(units // tile,), in_specs=[smem, smem] +...]
    ppermute x7, waiting for transfers between devices: 9.93 us -> 3.55 us  [over_tp(): return [array, lax.ppermute(array, 'tp', [(0, 1), (1, 0)])]]
    dynamic_update_slice x8 -> x0, local copies, waits for them, and re-layouts: 5.87 us -> none  [swap_finish(): lax.dynamic_update_slice_in_dim(joined, piece, (place ^ turn) * rows, axi...]
    convert_element_type x2 -> x0, other arithmetic: 5.4 us -> none  [contributions(): return (both[0].astype(f32) + other.astype(f32)).astype(bf16)]
    ppermute x2 -> x3, waiting for transfers between devices: 4.75 us -> 0.01 us  [contributions(): other = lax.ppermute(both[1], 'tp', [(0, 1), (1, 0)])]
    pallas_call x2 -> x3, Pallas kernels: 22.4 us -> 26.9 us  [down_rows(): pl.pallas_call(down_kernel, grid_spec=grid_spec, out_shape=jax.ShapeDtype...]
  transfers between devices with their start and end apart: 40 -> 41, of which waited for: 20 -> 18; matrix products, arithmetic and copies ran while one was open for 10% -> 11% of each run, Pallas kernels for 24% -> 35%
where the time goes in v1:
time: 346 us; the launch traced here: 345 us
  Pallas kernels  122 us (35%)
  waiting for transfers between devices  109 us (32%)
  starting transfers between devices  50.4 us (15%)
  local copies, waits for them, and re-layouts  31 us (9%)
  between operations  13.7 us (4%)
  other arithmetic  11.2 us (3%)
  matrix products  7.71 us (2%)
    ppermute x22, waiting for transfers between devices, partner(): lax.ppermute(array, 'inner', [(i, i ^ turn) for i in range(lax.axis_size(...  86 us
    pallas_call x1, Pallas kernels, mixer(): pl.pallas_call(functools.partial(mixer_kernel, first_group=first), grid=(...  32.2 us
    pallas_call x3, Pallas kernels, up_rows(): pl.pallas_call(up_kernel, grid=(units // tile,), in_specs=[smem, smem] +...  31 us
    ppermute x22, starting transfers between devices, partner(): lax.ppermute(array, 'inner', [(i, i ^ turn) for i in range(lax.axis_size(...  28.5 us
    pallas_call x3, Pallas kernels, down_rows(): pl.pallas_call(down_kernel, grid_spec=grid_spec, out_shape=jax.ShapeDtype...  26.9 us
    ppermute x6, starting transfers between devices, shifted(): return lax.ppermute(array, axis, pairs)  19.7 us
    pallas_call x1, Pallas kernels, per_device(): pl.pallas_call(gate_kernel, grid=(groups,), in_specs=[smem, rows_spec(wid...  9.52 us
    ppermute x6, waiting for transfers between devices, shifted(): return lax.ppermute(array, axis, pairs)  9.19 us
  transfers between devices with their start and end apart: 41, of which 18 were waited for; matrix products, arithmetic and copies ran while one was open for 11% of the time, Pallas kernels for 35%

profile of v1, /device:TPU:0, one launch (start us, length us, event | category | flops | bytes accessed | tf_op | source)
XLA Modules:
  0.0 344.8 jit_solution(9588048171239095219)
XLA Ops:
  7.9 3.0 collective-permute-start.2
  10.9 1.5 collective-permute-start.3
  15.3 4.5 %collective-permute-start = (bf16[8,2048]{1,0:T(8,128)(2,1)S(1)}, bf16[8,2048]{1,0:T(8,128)(2,1)S(1)}, u32[]{:S(2)}, u32[]{:S(2)}) collective-permute-start(bf16[8,2048]{1,0:T(8,128)(2,1)S(1)} %pad_maximum_fusion.2), channel_id=1, source_target_pairs={{0,2},{2,4},{4,6},{6,8},{8,10},{10,12},{12,14},{14,16},{16,18},{18... | collective-permute-start | bytes 98312 | tf_op jit(solution)/shard_map/ppermute | solution.py:31
  19.8 4.1 %collective-permute-done.1.high_value_ref.high_entry_ref.high_readout_ref = bf16[8,2048]{1,0:T(8,128)(2,1)S(1)} collective-permute-done((bf16[8,2048]{1,0:T(8,128)(2,1)S(1)}, bf16[8,2048]{1,0:T(8,128)(2,1)S(1)}, u32[]{:S(2)}, u32[]{:S(2)}) %collective-permute-start.1) | collective-permute-done | bytes 32800 | tf_op jit(solution)/shard_map/ppermute | solution.py:31
  30.1 1.6 constant_dynamic-update-slice_fusion.3
  31.7 32.2 %mixer.1 = (f32[768,1024]{1,0:T(8,128)}, bf16[768,512]{1,0:T(8,128)(2,1)}, f32[4,768,8]{2,1,0:T(8,128)}, bf16[4,2,4,48,256]{4,3,2,1,0:T(8,128)(2,1)}) custom-call(bf16[768,1024]{1,0:T(8,128)(2,1)} %value_ref.1, bf16[768,512]{1,0:T(8,128)(2,1)} %entry_ref.1, bf16[768,512]{1,0:T(8,128)(2,1)} %readout_ref.1, bf16[8,2048]{1,0:T(8,128)(2,1)} %copy-done.12, ...), custom_call_target="tpu_custom_call" | custom-call | tf_op jit(solution)/shard_map/mixer/pallas_call | solution.py:617
  63.9 2.2 dynamic-slice_bitcast_fusion.1
  66.1 2.3 collective-permute-start.5
  69.9 4.4 %collective-permute-done.5.refs_1_ = bf16[2,4,48,256]{3,2,1,0:T(8,128)(2,1)S(1)} collective-permute-done((bf16[2,4,48,256]{3,2,1,0:T(8,128)(2,1)}, bf16[2,4,48,256]{3,2,1,0:T(8,128)(2,1)S(1)}, u32[]{:S(2)}, u32[]{:S(2)}) %collective-permute-start.5) | collective-permute-done | bytes 196640 | tf_op jit(solution)/shard_map/ppermute | solution.py:39
  74.3 5.0 %collective-permute-done.6.refs_2_ = bf16[2,4,48,256]{3,2,1,0:T(8,128)(2,1)S(1)} collective-permute-done((bf16[2,4,48,256]{3,2,1,0:T(8,128)(2,1)}, bf16[2,4,48,256]{3,2,1,0:T(8,128)(2,1)S(1)}, u32[]{:S(2)}, u32[]{:S(2)}) %collective-permute-start.6) | collective-permute-done | bytes 196640 | tf_op jit(solution)/shard_map/ppermute | solution.py:39
  80.0 3.1 whole.1
  85.7 5.2 %collective-permute-start.8 = (bf16[4,48,256]{2,1,0:T(8,128)(2,1)}, bf16[4,48,256]{2,1,0:T(8,128)(2,1)}, u32[]{:S(2)}, u32[]{:S(2)}) collective-permute-start(bf16[4,48,256]{2,1,0:T(8,128)(2,1)} %get-tuple-element.44), channel_id=1, source_target_pairs={{0,8},{8,16},{16,24},{1,9},{9,17},{17,25},{2,10},{10,18},{18,26},{... | collective-permute-start | bytes 294920 | tf_op jit(solution)/shard_map/ppermute | solution.py:31
  90.9 6.1 %collective-permute-start.9 = (bf16[4,48,256]{2,1,0:T(8,128)(2,1)}, bf16[4,48,256]{2,1,0:T(8,128)(2,1)}, u32[]{:S(2)}, u32[]{:S(2)}) collective-permute-start(bf16[4,48,256]{2,1,0:T(8,128)(2,1)} %get-tuple-element.44), channel_id=1, source_target_pairs={{0,16},{8,24},{1,17},{9,25},{2,18},{10,26},{3,19},{11,27},{4,20},{... | collective-permute-start | bytes 294920 | tf_op jit(solution)/shard_map/ppermute | solution.py:31
  97.0 2.1 dynamic-slice_bitcast_fusion
  100.5 5.0 %collective-permute-done.11.refs_7_ = bf16[4,48,256]{2,1,0:T(8,128)(2,1)} collective-permute-done((bf16[4,48,256]{2,1,0:T(8,128)(2,1)}, bf16[4,48,256]{2,1,0:T(8,128)(2,1)}, u32[]{:S(2)}, u32[]{:S(2)}) %collective-permute-start.11) | collective-permute-done | bytes 98336 | tf_op jit(solution)/shard_map/ppermute | solution.py:31
  106.7 3.3 arrive.1
  109.9 1.8 slice_bitcast_fusion.4
  115.2 1.6 constant_dynamic-update-slice_fusion.2.refs_2_
  119.0 5.8 %collective-permute-done.13.refs_7_ = bf16[4,32,512]{2,1,0:T(8,128)(2,1)} collective-permute-done((bf16[4,32,512]{2,1,0:T(8,128)(2,1)S(1)}, bf16[4,32,512]{2,1,0:T(8,128)(2,1)}, u32[]{:S(2)}, u32[]{:S(2)}) %collective-permute-start.13) | collective-permute-done | bytes 131104 | tf_op jit(solution)/shard_map/ppermute | solution.py:39
  124.8 9.5 %gate.1 = bf16[768,1024]{1,0:T(8,128)(2,1)} custom-call(s32[1]{0:T(128)} %bitcast.1.place_ref.inner_ref, f32[768,1024]{1,0:T(8,128)} %get-tuple-element.40.refs_0_, bf16[768,512]{1,0:T(8,128)(2,1)} %get-tuple-element.41.refs_1_, f32[4,768,8]{2,1,0:T(8,128)} %get-tuple-element.42.refs_2_, bf16[768,1024]{1,0:T(8,128)(2,1)} %refs_3_.1, f32[1,1024]{1,0:T(1,128)} %bitcast.55, ...), custom_call_target="tpu_custom_call" | custom-call | tf_op jit(solution)/shard_map/gate/pallas_call | solution.py:698
  134.3 7.7 %convolution_convert_fusion.refs_0_ = bf16[768,2048]{1,0:T(8,128)(2,1)} fusion(bf16[768,1024]{1,0:T(8,128)(2,1)} %gate.1, bf16[1024,2048]{1,0:T(8,128)(2,1)} %param.32), kind=kOutput, calls=%fused_computation | convolution fusion | flops 3222798336 | bytes 8912896 | tf_op jit(solution)/shard_map/dot_general | solution.py:711
  142.1 2.3 pad_maximum_fusion.1
  144.4 3.5 %collective-permute-done.17.refs_1_ = bf16[768,2048]{1,0:T(8,128)(2,1)S(1)} collective-permute-done((bf16[768,2048]{1,0:T(8,128)(2,1)}, bf16[768,2048]{1,0:T(8,128)(2,1)S(1)}, u32[]{:S(2)}, u32[]{:S(2)}) %collective-permute-start.17) | collective-permute-done | bytes 3145760 | tf_op jit(solution)/shard_map/ppermute | solution.py:46
  147.9 1.6 copy-done.5
  149.6 8.2 %norm_rows.1 = (bf16[768,1024]{1,0:T(8,128)(2,1)}, bf16[768,1024]{1,0:T(8,128)(2,1)}) custom-call(s32[1]{0:T(128)} %bitcast.place_ref, bf16[768,2048]{1,0:T(8,128)(2,1)} %convolution_convert_fusion.refs_0_, bf16[768,2048]{1,0:T(8,128)(2,1)} %copy-done.5, bf16[768,2048]{1,0:T(8,128)(2,1)} %copy-done.1, f32[1,2048]{1,0:T(1,128)} %copy-done.17), custom_call_target="tpu_custom_call" | custom-call | tf_op jit(solution)/shard_map/norm_rows/pallas_call | solution.py:528
  157.8 2.7 collective-permute-start.19
  160.6 8.6 %up_rows.3.refs_0_ = bf16[768,1024]{1,0:T(8,128)(2,1)} custom-call(s32[1]{0:T(128)} %bitcast.place_ref, s32[1]{0:T(128)} %bitcast.1.place_ref.inner_ref, bf16[768,1024]{1,0:T(8,128)(2,1)} %get-tuple-element.52.refs_0_, bf16[768,1024]{1,0:T(8,128)(2,1)} %get-tuple-element.53.refs_1_, bf16[4,4,128,1024]{3,2,1,0:T(8,128)(2,1)} %bitcast.45), custom_call_target="tpu_custom_call" | custom-call | tf_op jit(solution)/shard_map/up_rows/pallas_call | solution.py:422
  169.2 25.3 %collective-permute-done.18.refs_0_ = bf16[768,1024]{1,0:T(8,128)(2,1)S(1)} collective-permute-done((bf16[768,1024]{1,0:T(8,128)(2,1)}, bf16[768,1024]{1,0:T(8,128)(2,1)S(1)}, u32[]{:S(2)}, u32[]{:S(2)}) %collective-permute-start.18) | collective-permute-done | bytes 1572896 | tf_op jit(solution)/shard_map/ppermute | solution.py:39
  197.7 2.1 collective-permute-start.26
  202.4 13.8 %up_rows.4.refs_0_ = bf16[1536,1024]{1,0:T(8,128)(2,1)} custom-call(s32[1]{0:T(128)} %bitcast.place_ref, s32[1]{0:T(128)} %bitcast.1.place_ref.inner_ref, bf16[768,1024]{1,0:T(8,128)(2,1)} %copy-done.3, bf16[768,1024]{1,0:T(8,128)(2,1)} %copy-done.6, bf16[768,1024]{1,0:T(8,128)(2,1)} %copy-done.4, bf16[768,1024]{1,0:T(8,128)(2,1)} %collective-permute-done.25.refs_3_, ...), custom_call_target="tpu_custom_call" | custom-call | tf_op jit(solution)/shard_map/up_rows/pallas_call | solution.py:422
  219.5 8.7 %all-gather.7.cloned.1.call-done = bf16[16,128,1024]{2,1,0:T(8,128)(2,1)} async-done(((bf16[4,128,1024]{2,1,0:T(8,128)(2,1)}), bf16[16,128,1024]{2,1,0:T(8,128)(2,1)}) %all-gather.7.cloned.1.call-update) | async-done | bytes 4194320 | tf_op jit(solution)/shard_map/all_gather | solution.py:691
  228.2 11.7 %down_rows.4.here_ref = bf16[2,1536,1024]{2,1,0:T(8,128)(2,1)} custom-call(s32[1]{0:T(128)} %bitcast.place_ref, s32[1]{0:T(128)} %bitcast.1.place_ref.inner_ref, bf16[1536,1024]{1,0:T(8,128)(2,1)} %up_rows.4.refs_0_, bf16[4,4,128,1024]{3,2,1,0:T(8,128)(2,1)} %bitcast.48), custom_call_target="tpu_custom_call" | custom-call | tf_op jit(solution)/shard_map/down_rows/pallas_call | solution.py:468
  239.9 3.9 %slice_bitcast_fusion = bf16[1536,1024]{1,0:T(8,128)(2,1)} fusion(bf16[2,1536,1024]{2,1,0:T(8,128)(2,1)} %down_rows.4.here_ref), kind=kLoop, calls=%fused_computation.1 | loop fusion | bytes 6291456 | tf_op jit(solution)/shard_map/squeeze | solution.py:732
  245.6 8.5 %up_rows.5.refs_0_ = bf16[768,1024]{1,0:T(8,128)(2,1)} custom-call(s32[1]{0:T(128)} %bitcast.place_ref, s32[1]{0:T(128)} %bitcast.1.place_ref.inner_ref, bf16[384,1024]{1,0:T(8,128)(2,1)} %collective-permute-done.26.refs_0_, bf16[384,1024]{1,0:T(8,128)(2,1)} %copy-done.7, bf16[384,1024]{1,0:T(8,128)(2,1)} %collective-permute-done.27.refs_2_, ...), custom_call_target="tpu_custom_call" | custom-call | tf_op jit(solution)/shard_map/up_rows/pallas_call | solution.py:422
  254.1 7.6 %down_rows.5.here_ref = bf16[2,768,1024]{2,1,0:T(8,128)(2,1)} custom-call(s32[1]{0:T(128)} %bitcast.place_ref, s32[1]{0:T(128)} %bitcast.1.place_ref.inner_ref, bf16[768,1024]{1,0:T(8,128)(2,1)} %up_rows.5.refs_0_, bf16[4,4,128,1024]{3,2,1,0:T(8,128)(2,1)} %bitcast.49), custom_call_target="tpu_custom_call" | custom-call | tf_op jit(solution)/shard_map/down_rows/pallas_call | solution.py:468
  261.7 2.7 slice_bitcast_fusion.1
  264.9 7.6 %down_rows.3 = bf16[2,768,1024]{2,1,0:T(8,128)(2,1)} custom-call(s32[1]{0:T(128)} %bitcast.place_ref, s32[1]{0:T(128)} %bitcast.1.place_ref.inner_ref, bf16[768,1024]{1,0:T(8,128)(2,1)} %up_rows.3.refs_0_, bf16[4,4,128,1024]{3,2,1,0:T(8,128)(2,1)} %bitcast.50), custom_call_target="tpu_custom_call" | custom-call | tf_op jit(solution)/shard_map/down_rows/pallas_call | solution.py:468
  272.5 3.4 summed_pieces.3
  278.5 1.5 collective-permute-start.36
  279.9 4.7 %summed_pieces.2 = (bf16[384,1024]{1,0:T(8,128)(2,1)}, bf16[384,1024]{1,0:T(8,128)(2,1)}, bf16[384,1024]{1,0:T(8,128)(2,1)}, bf16[384,1024]{1,0:T(8,128)(2,1)}) custom-call(bf16[2,1536,1024]{2,1,0:T(8,128)(2,1)} %down_rows.4.here_ref, bf16[1536,1024]{1,0:T(8,128)(2,1)} %collective-permute-done.28.other_ref), custom_call_target="tpu_custom_call" | custom-call | tf_op jit(solution)/shard_map/summed_pieces/pallas_call | solution.py:487
  286.0 10.7 %collective-permute-done.32 = bf16[384,1024]{1,0:T(8,128)(2,1)} collective-permute-done((bf16[384,1024]{1,0:T(8,128)(2,1)}, bf16[384,1024]{1,0:T(8,128)(2,1)}, u32[]{:S(2)}, u32[]{:S(2)}) %collective-permute-start.32) | collective-permute-done | bytes 786464 | tf_op jit(solution)/shard_map/ppermute | solution.py:39
  296.7 1.7 add.89
  299.6 1.7 add.91
  301.3 1.5 collective-permute-start.37
  302.9 13.1 %collective-permute-done.34 = bf16[384,1024]{1,0:T(8,128)(2,1)S(1)} collective-permute-done((bf16[384,1024]{1,0:T(8,128)(2,1)}, bf16[384,1024]{1,0:T(8,128)(2,1)S(1)}, u32[]{:S(2)}, u32[]{:S(2)}) %collective-permute-start.34) | collective-permute-done | bytes 786464 | tf_op jit(solution)/shard_map/ppermute | solution.py:39
  315.9 16.4 %collective-permute-done.33 = bf16[384,1024]{1,0:T(8,128)(2,1)S(1)} collective-permute-done((bf16[384,1024]{1,0:T(8,128)(2,1)S(1)}, bf16[384,1024]{1,0:T(8,128)(2,1)S(1)}, u32[]{:S(2)}, u32[]{:S(2)}) %collective-permute-start.33) | collective-permute-done | bytes 786464 | tf_op jit(solution)/shard_map/ppermute | solution.py:39
  332.3 2.7 fusion.5
  336.4 1.6 multiply_convert_fusion
  (129 shorter events, 40.9 us)
Async XLA Ops:
  6.5 19.2 %copy-start.19 = (f32[1024]{0:T(1024)S(1)}, f32[1024]{0:T(1024)}, u32[]{:S(2)}) copy-start(f32[1024]{0:T(1024)} %param.34) | copy-start | bytes 12292
  6.5 19.7 %copy-start.16 = (s32[12288]{0:T(1024)S(1)}, s32[12288]{0:T(1024)}, u32[]{:S(2)}) copy-start(s32[12288]{0:T(1024)} %param.25) | copy-start | bytes 147460
  6.5 21.4 %copy-start.15 = (f32[768,16]{0,1:T(8,128)S(1)}, f32[768,16]{0,1:T(8,128)}, u32[]{:S(2)}) copy-start(f32[768,16]{0,1:T(8,128)} %param.24) | copy-start | bytes 147460
  6.5 154.0 %all-gather.5.cloned.1.call-start = ((), (), s32[]{:S(2)}) async-start(), calls=%async_computation | async-start | bytes 5242880 | tf_op jit(solution)/shard_map/all_gather | solution.py:579
  6.5 22.3 %copy-start.18 = (bf16[768,16]{0,1:T(8,128)(2,1)S(1)}, bf16[768,16]{0,1:T(8,128)(2,1)}, u32[]{:S(2)}) copy-start(bf16[768,16]{0,1:T(8,128)(2,1)} %param.23) | copy-start | bytes 73732
  7.9 16.1 %collective-permute-start.2 = (bf16[128,1024]{1,0:T(8,128)(2,1)S(1)}, bf16[128,1024]{1,0:T(8,128)(2,1)S(1)}, u32[]{:S(2)}, u32[]{:S(2)}) collective-permute-start(bf16[128,1024]{1,0:T(8,128)(2,1)S(1)} %get-tuple-element.83), channel_id=1, source_target_pairs={{0,2},{2,0},{4,6},{6,4},{1,3},{3,1},{5,7},{7,5},{8,10},{10,8},{12,... | collective-permute-start | bytes 786440 | tf_op jit(solution)/shard_map/ppermute | solution.py:39
  10.9 13.2 %collective-permute-start.3 = (bf16[128,1024]{1,0:T(8,128)(2,1)S(1)}, bf16[128,1024]{1,0:T(8,128)(2,1)S(1)}, u32[]{:S(2)}, u32[]{:S(2)}) collective-permute-start(bf16[128,1024]{1,0:T(8,128)(2,1)S(1)} %get-tuple-element.85), channel_id=1, source_target_pairs={{0,4},{2,6},{4,0},{6,2},{1,5},{3,7},{5,1},{7,3},{8,12},{10,14},{12... | collective-permute-start | bytes 786440 | tf_op jit(solution)/shard_map/ppermute | solution.py:39
  12.4 12.0 %collective-permute-start.4 = (bf16[128,1024]{1,0:T(8,128)(2,1)S(1)}, bf16[128,1024]{1,0:T(8,128)(2,1)S(1)}, u32[]{:S(2)}, u32[]{:S(2)}) collective-permute-start(bf16[128,1024]{1,0:T(8,128)(2,1)S(1)} %get-tuple-element.82), channel_id=1, source_target_pairs={{0,6},{2,4},{4,2},{6,0},{1,7},{3,5},{5,3},{7,1},{8,14},{10,12},{12... | collective-permute-start | bytes 786440 | tf_op jit(solution)/shard_map/ppermute | solution.py:39
  14.0 10.0 %collective-permute-start.1 = (bf16[8,2048]{1,0:T(8,128)(2,1)S(1)}, bf16[8,2048]{1,0:T(8,128)(2,1)S(1)}, u32[]{:S(2)}, u32[]{:S(2)}) collective-permute-start(bf16[8,2048]{1,0:T(8,128)(2,1)S(1)} %pad_maximum_fusion.3), channel_id=1, source_target_pairs={{2,0},{4,2},{6,4},{8,6},{10,8},{12,10},{14,12},{16,14},{18,16},{20... | collective-permute-start | bytes 98312 | tf_op jit(solution)/shard_map/ppermute | solution.py:31
  15.3 8.7 %collective-permute-start = (bf16[8,2048]{1,0:T(8,128)(2,1)S(1)}, bf16[8,2048]{1,0:T(8,128)(2,1)S(1)}, u32[]{:S(2)}, u32[]{:S(2)}) collective-permute-start(bf16[8,2048]{1,0:T(8,128)(2,1)S(1)} %pad_maximum_fusion.2), channel_id=1, source_target_pairs={{0,2},{2,4},{4,6},{6,8},{8,10},{10,12},{12,14},{14,16},{16,18},{18... | collective-permute-start | bytes 98312 | tf_op jit(solution)/shard_map/ppermute | solution.py:31
  25.6 202.6 %all-gather.7.cloned.1.call-start = ((), (), s32[]{:S(2)}) async-start(), calls=%async_computation.1 | async-start | bytes 5242880 | tf_op jit(solution)/shard_map/all_gather | solution.py:691
  25.6 88.7 %collective-permute-start.15 = (bf16[768,1024]{1,0:T(8,128)(2,1)}, bf16[768,1024]{1,0:T(8,128)(2,1)}, u32[]{:S(2)}, u32[]{:S(2)}) collective-permute-start(bf16[768,1024]{1,0:T(8,128)(2,1)} %param.33), channel_id=1, source_target_pairs={{0,1},{1,0},{2,3},{3,2},{4,5},{5,4},{6,7},{7,6},{8,9},{9,8},{10,11... | collective-permute-start | bytes 4718600 | tf_op jit(solution)/shard_map/ppermute | solution.py:46
  25.7 44.1 %collective-permute-start.16 = (f32[1,1024]{1,0:T(1,128)S(1)}, f32[1,1024]{1,0:T(1,128)S(1)}, u32[]{:S(2)}, u32[]{:S(2)}) collective-permute-start(f32[1,1024]{1,0:T(1,128)S(1)} %bitcast.56), channel_id=1, source_target_pairs={{0,1},{1,0},{2,3},{3,2},{4,5},{5,4},{6,7},{7,6},{8,9},{9,8},{10,11... | collective-permute-start | bytes 12296 | tf_op jit(solution)/shard_map/ppermute | solution.py:46
  66.1 8.3 %collective-permute-start.5 = (bf16[2,4,48,256]{3,2,1,0:T(8,128)(2,1)}, bf16[2,4,48,256]{3,2,1,0:T(8,128)(2,1)S(1)}, u32[]{:S(2)}, u32[]{:S(2)}) collective-permute-start(bf16[2,4,48,256]{3,2,1,0:T(8,128)(2,1)} %get-tuple-element.88), channel_id=1, source_target_pairs={{0,2},{2,0},{4,6},{6,4},{1,3},{3,1},{5,7},{7,5},{8,10},{10,8},{12,... | collective-permute-start | bytes 589832 | tf_op jit(solution)/shard_map/ppermute | solution.py:39
  68.3 11.0 %collective-permute-start.6 = (bf16[2,4,48,256]{3,2,1,0:T(8,128)(2,1)}, bf16[2,4,48,256]{3,2,1,0:T(8,128)(2,1)S(1)}, u32[]{:S(2)}, u32[]{:S(2)}) collective-permute-start(bf16[2,4,48,256]{3,2,1,0:T(8,128)(2,1)} %get-tuple-element.87), channel_id=1, source_target_pairs={{0,4},{2,6},{4,0},{6,2},{1,5},{3,7},{5,1},{7,3},{8,12},{10,14},{12... | collective-permute-start | bytes 589832 | tf_op jit(solution)/shard_map/ppermute | solution.py:39
  69.1 10.2 %collective-permute-start.7 = (bf16[2,4,48,256]{3,2,1,0:T(8,128)(2,1)}, bf16[2,4,48,256]{3,2,1,0:T(8,128)(2,1)}, u32[]{:S(2)}, u32[]{:S(2)}) collective-permute-start(bf16[2,4,48,256]{3,2,1,0:T(8,128)(2,1)} %get-tuple-element.86), channel_id=1, source_target_pairs={{0,6},{2,4},{4,2},{6,0},{1,7},{3,5},{5,3},{7,1},{8,14},{10,12},{12... | collective-permute-start | bytes 589832 | tf_op jit(solution)/shard_map/ppermute | solution.py:39
  69.9 72.2 %copy-start.17 = (f32[1,2048]{1,0:T(1,128)}, f32[1,2048]{1,0:T(1,128)S(1)}, u32[]{:S(2)}) copy-start(f32[1,2048]{1,0:T(1,128)S(1)} %constant_dynamic-update-slice_fusion.refs_3_) | copy-start | bytes 24580
  83.1 16.0 %collective-permute-start.10 = (bf16[4,48,256]{2,1,0:T(8,128)(2,1)}, bf16[4,48,256]{2,1,0:T(8,128)(2,1)S(1)}, u32[]{:S(2)}, u32[]{:S(2)}) collective-permute-start(bf16[4,48,256]{2,1,0:T(8,128)(2,1)} %get-tuple-element.45), channel_id=1, source_target_pairs={{8,0},{16,8},{24,16},{9,1},{17,9},{25,17},{10,2},{18,10},{26,18},{... | collective-permute-start | bytes 294920 | tf_op jit(solution)/shard_map/ppermute | solution.py:31
  84.4 21.2 %collective-permute-start.11 = (bf16[4,48,256]{2,1,0:T(8,128)(2,1)}, bf16[4,48,256]{2,1,0:T(8,128)(2,1)}, u32[]{:S(2)}, u32[]{:S(2)}) collective-permute-start(bf16[4,48,256]{2,1,0:T(8,128)(2,1)} %get-tuple-element.45), channel_id=1, source_target_pairs={{16,0},{24,8},{17,1},{25,9},{18,2},{26,10},{19,3},{27,11},{20,4},{... | collective-permute-start | bytes 294920 | tf_op jit(solution)/shard_map/ppermute | solution.py:31
  85.7 21.0 %collective-permute-start.8 = (bf16[4,48,256]{2,1,0:T(8,128)(2,1)}, bf16[4,48,256]{2,1,0:T(8,128)(2,1)}, u32[]{:S(2)}, u32[]{:S(2)}) collective-permute-start(bf16[4,48,256]{2,1,0:T(8,128)(2,1)} %get-tuple-element.44), channel_id=1, source_target_pairs={{0,8},{8,16},{16,24},{1,9},{9,17},{17,25},{2,10},{10,18},{18,26},{... | collective-permute-start | bytes 294920 | tf_op jit(solution)/shard_map/ppermute | solution.py:31
  90.9 15.8 %collective-permute-start.9 = (bf16[4,48,256]{2,1,0:T(8,128)(2,1)}, bf16[4,48,256]{2,1,0:T(8,128)(2,1)}, u32[]{:S(2)}, u32[]{:S(2)}) collective-permute-start(bf16[4,48,256]{2,1,0:T(8,128)(2,1)} %get-tuple-element.44), channel_id=1, source_target_pairs={{0,16},{8,24},{1,17},{9,25},{2,18},{10,26},{3,19},{11,27},{4,20},{... | collective-permute-start | bytes 294920 | tf_op jit(solution)/shard_map/ppermute | solution.py:31
  99.1 43.0 %collective-permute-start.20 = (bf16[128,1024]{1,0:T(8,128)(2,1)}, bf16[128,1024]{1,0:T(8,128)(2,1)}, u32[]{:S(2)}, u32[]{:S(2)}) collective-permute-start(bf16[128,1024]{1,0:T(8,128)(2,1)} %get-tuple-element.81), channel_id=1, source_target_pairs={{0,2},{2,0},{4,6},{6,4},{1,3},{3,1},{5,7},{7,5},{8,10},{10,8},{12,... | collective-permute-start | bytes 786440 | tf_op jit(solution)/shard_map/ppermute | solution.py:39
  105.6 36.5 %collective-permute-start.21 = (bf16[128,1024]{1,0:T(8,128)(2,1)}, bf16[128,1024]{1,0:T(8,128)(2,1)}, u32[]{:S(2)}, u32[]{:S(2)}) collective-permute-start(bf16[128,1024]{1,0:T(8,128)(2,1)} %get-tuple-element.80), channel_id=1, source_target_pairs={{0,4},{2,6},{4,0},{6,2},{1,5},{3,7},{5,1},{7,3},{8,12},{10,14},{12... | collective-permute-start | bytes 786440 | tf_op jit(solution)/shard_map/ppermute | solution.py:39
  111.7 6.1 %collective-permute-start.12 = (bf16[4,32,512]{2,1,0:T(8,128)(2,1)S(1)}, bf16[4,32,512]{2,1,0:T(8,128)(2,1)S(1)}, u32[]{:S(2)}, u32[]{:S(2)}) collective-permute-start(bf16[4,32,512]{2,1,0:T(8,128)(2,1)S(1)} %get-tuple-element.96), channel_id=1, source_target_pairs={{0,2},{2,0},{4,6},{6,4},{1,3},{3,1},{5,7},{7,5},{8,10},{10,8},{12,... | collective-permute-start | bytes 393224 | tf_op jit(solution)/shard_map/ppermute | solution.py:39
  113.0 11.8 %collective-permute-start.13 = (bf16[4,32,512]{2,1,0:T(8,128)(2,1)S(1)}, bf16[4,32,512]{2,1,0:T(8,128)(2,1)}, u32[]{:S(2)}, u32[]{:S(2)}) collective-permute-start(bf16[4,32,512]{2,1,0:T(8,128)(2,1)S(1)} %get-tuple-element.95), channel_id=1, source_target_pairs={{0,4},{2,6},{4,0},{6,2},{1,5},{3,7},{5,1},{7,3},{8,12},{10,14},{12... | collective-permute-start | bytes 393224 | tf_op jit(solution)/shard_map/ppermute | solution.py:39
  114.3 10.5 %collective-permute-start.14 = (bf16[4,32,512]{2,1,0:T(8,128)(2,1)S(1)}, bf16[4,32,512]{2,1,0:T(8,128)(2,1)}, u32[]{:S(2)}, u32[]{:S(2)}) collective-permute-start(bf16[4,32,512]{2,1,0:T(8,128)(2,1)S(1)} %get-tuple-element.94), channel_id=1, source_target_pairs={{0,6},{2,4},{4,2},{6,0},{1,7},{3,5},{5,3},{7,1},{8,14},{10,12},{12... | collective-permute-start | bytes 393224 | tf_op jit(solution)/shard_map/ppermute | solution.py:39
  117.8 24.3 %collective-permute-start.22 = (bf16[128,1024]{1,0:T(8,128)(2,1)}, bf16[128,1024]{1,0:T(8,128)(2,1)}, u32[]{:S(2)}, u32[]{:S(2)}) collective-permute-start(bf16[128,1024]{1,0:T(8,128)(2,1)} %get-tuple-element.79), channel_id=1, source_target_pairs={{0,6},{2,4},{4,2},{6,0},{1,7},{3,5},{5,3},{7,1},{8,14},{10,12},{12... | collective-permute-start | bytes 786440 | tf_op jit(solution)/shard_map/ppermute | solution.py:39
  142.1 5.9 %collective-permute-start.17 = (bf16[768,2048]{1,0:T(8,128)(2,1)}, bf16[768,2048]{1,0:T(8,128)(2,1)S(1)}, u32[]{:S(2)}, u32[]{:S(2)}) collective-permute-start(bf16[768,2048]{1,0:T(8,128)(2,1)} %convolution_convert_fusion.refs_0_), channel_id=1, source_target_pairs={{0,1},{1,0},{2,3},{3,2},{4,5},{5,4},{6,7},{7,6},{8,9},{9,8},{10,11... | collective-permute-start | bytes 9437192 | tf_op jit(solution)/shard_map/ppermute | solution.py:46
  157.8 36.7 %collective-permute-start.18 = (bf16[768,1024]{1,0:T(8,128)(2,1)}, bf16[768,1024]{1,0:T(8,128)(2,1)S(1)}, u32[]{:S(2)}, u32[]{:S(2)}) collective-permute-start(bf16[768,1024]{1,0:T(8,128)(2,1)} %get-tuple-element.52.refs_0_), channel_id=1, source_target_pairs={{0,2},{2,0},{4,6},{6,4},{1,3},{3,1},{5,7},{7,5},{8,10},{10,8},{12,... | collective-permute-start | bytes 4718600 | tf_op jit(solution)/shard_map/ppermute | solution.py:39
  157.8 37.5 %collective-permute-start.19 = (bf16[768,1024]{1,0:T(8,128)(2,1)}, bf16[768,1024]{1,0:T(8,128)(2,1)S(1)}, u32[]{:S(2)}, u32[]{:S(2)}) collective-permute-start(bf16[768,1024]{1,0:T(8,128)(2,1)} %get-tuple-element.52.refs_0_), channel_id=1, source_target_pairs={{0,4},{2,6},{4,0},{6,2},{1,5},{3,7},{5,1},{7,3},{8,12},{10,14},{12... | collective-permute-start | bytes 4718600 | tf_op jit(solution)/shard_map/ppermute | solution.py:39
  195.3 5.8 %collective-permute-start.24 = (bf16[768,1024]{1,0:T(8,128)(2,1)S(1)}, bf16[768,1024]{1,0:T(8,128)(2,1)S(1)}, u32[]{:S(2)}, u32[]{:S(2)}) collective-permute-start(bf16[768,1024]{1,0:T(8,128)(2,1)S(1)} %collective-permute-done.18.refs_0_), channel_id=1, source_target_pairs={{0,1},{1,0},{2,3},{3,2},{4,5},{5,4},{6,7},{7,6},{8,9},{9,8},{10,11... | collective-permute-start | bytes 4718600 | tf_op jit(solution)/shard_map/ppermute | solution.py:46
  195.3 7.0 %collective-permute-start.25 = (bf16[768,1024]{1,0:T(8,128)(2,1)S(1)}, bf16[768,1024]{1,0:T(8,128)(2,1)}, u32[]{:S(2)}, u32[]{:S(2)}) collective-permute-start(bf16[768,1024]{1,0:T(8,128)(2,1)S(1)} %collective-permute-done.19.refs_2_), channel_id=1, source_target_pairs={{0,1},{1,0},{2,3},{3,2},{4,5},{5,4},{6,7},{7,6},{8,9},{9,8},{10,11... | collective-permute-start | bytes 4718600 | tf_op jit(solution)/shard_map/ppermute | solution.py:46
  197.7 19.8 %collective-permute-start.26 = (bf16[384,1024]{1,0:T(8,128)(2,1)}, bf16[384,1024]{1,0:T(8,128)(2,1)}, u32[]{:S(2)}, u32[]{:S(2)}) collective-permute-start(bf16[384,1024]{1,0:T(8,128)(2,1)} %slice.70), channel_id=1, source_target_pairs={{0,4},{2,6},{4,0},{6,2},{1,5},{3,7},{5,1},{7,3},{8,12},{10,14},{12... | collective-permute-start | bytes 2359304 | tf_op jit(solution)/shard_map/ppermute | solution.py:39
  199.9 19.2 %collective-permute-start.27 = (bf16[384,1024]{1,0:T(8,128)(2,1)}, bf16[384,1024]{1,0:T(8,128)(2,1)}, u32[]{:S(2)}, u32[]{:S(2)}) collective-permute-start(bf16[384,1024]{1,0:T(8,128)(2,1)} %slice.71), channel_id=1, source_target_pairs={{0,2},{2,0},{4,6},{6,4},{1,3},{3,1},{5,7},{7,5},{8,10},{10,8},{12,... | collective-permute-start | bytes 2359304 | tf_op jit(solution)/shard_map/ppermute | solution.py:39
  219.0 24.7 %collective-permute-start.29 = (bf16[384,1024]{1,0:T(8,128)(2,1)}, bf16[384,1024]{1,0:T(8,128)(2,1)S(1)}, u32[]{:S(2)}, u32[]{:S(2)}) collective-permute-start(bf16[384,1024]{1,0:T(8,128)(2,1)} %collective-permute-done.26.refs_0_), channel_id=1, source_target_pairs={{0,1},{1,0},{2,3},{3,2},{4,5},{5,4},{6,7},{7,6},{8,9},{9,8},{10,11... | collective-permute-start | bytes 2359304 | tf_op jit(solution)/shard_map/ppermute | solution.py:46
  219.0 24.8 %collective-permute-start.30 = (bf16[384,1024]{1,0:T(8,128)(2,1)}, bf16[384,1024]{1,0:T(8,128)(2,1)S(1)}, u32[]{:S(2)}, u32[]{:S(2)}) collective-permute-start(bf16[384,1024]{1,0:T(8,128)(2,1)} %collective-permute-done.27.refs_2_), channel_id=1, source_target_pairs={{0,1},{1,0},{2,3},{3,2},{4,5},{5,4},{6,7},{7,6},{8,9},{9,8},{10,11... | collective-permute-start | bytes 2359304 | tf_op jit(solution)/shard_map/ppermute | solution.py:46
  243.8 36.2 %collective-permute-start.28 = (bf16[1536,1024]{1,0:T(8,128)(2,1)}, bf16[1536,1024]{1,0:T(8,128)(2,1)}, u32[]{:S(2)}, u32[]{:S(2)}) collective-permute-start(bf16[1536,1024]{1,0:T(8,128)(2,1)} %slice_bitcast_fusion), channel_id=1, source_target_pairs={{0,1},{1,0},{2,3},{3,2},{4,5},{5,4},{6,7},{7,6},{8,9},{9,8},{10,11... | collective-permute-start | bytes 9437192 | tf_op jit(solution)/shard_map/ppermute | solution.py:732
  264.4 8.1 %collective-permute-start.31 = (bf16[768,1024]{1,0:T(8,128)(2,1)}, bf16[768,1024]{1,0:T(8,128)(2,1)}, u32[]{:S(2)}, u32[]{:S(2)}) collective-permute-start(bf16[768,1024]{1,0:T(8,128)(2,1)} %slice_bitcast_fusion.1), channel_id=1, source_target_pairs={{0,1},{1,0},{2,3},{3,2},{4,5},{5,4},{6,7},{7,6},{8,9},{9,8},{10,11... | collective-permute-start | bytes 4718600 | tf_op jit(solution)/shard_map/ppermute | solution.py:732
  276.0 20.7 %collective-permute-start.32 = (bf16[384,1024]{1,0:T(8,128)(2,1)}, bf16[384,1024]{1,0:T(8,128)(2,1)}, u32[]{:S(2)}, u32[]{:S(2)}) collective-permute-start(bf16[384,1024]{1,0:T(8,128)(2,1)} %get-tuple-element.66), channel_id=1, source_target_pairs={{0,4},{2,6},{4,0},{6,2},{1,5},{3,7},{5,1},{7,3},{8,12},{10,14},{12... | collective-permute-start | bytes 2359304 | tf_op jit(solution)/shard_map/ppermute | solution.py:39
  278.5 24.4 %collective-permute-start.23 = (bf16[768,1024]{1,0:T(8,128)(2,1)}, bf16[768,1024]{1,0:T(8,128)(2,1)}, u32[]{:S(2)}, u32[]{:S(2)}) collective-permute-start(bf16[768,1024]{1,0:T(8,128)(2,1)} %slice_bitcast_fusion.2), channel_id=1, source_target_pairs={{0,1},{1,0},{2,3},{3,2},{4,5},{5,4},{6,7},{7,6},{8,9},{9,8},{10,11... | collective-permute-start | bytes 4718600 | tf_op jit(solution)/shard_map/ppermute | solution.py:732
  278.5 21.2 %collective-permute-start.36 = (bf16[384,1024]{1,0:T(8,128)(2,1)}, bf16[384,1024]{1,0:T(8,128)(2,1)}, u32[]{:S(2)}, u32[]{:S(2)}) collective-permute-start(bf16[384,1024]{1,0:T(8,128)(2,1)} %get-tuple-element.70), channel_id=1, source_target_pairs={{0,2},{2,0},{4,6},{6,4},{1,3},{3,1},{5,7},{7,5},{8,10},{10,8},{12,... | collective-permute-start | bytes 2359304 | tf_op jit(solution)/shard_map/ppermute | solution.py:39
  284.6 47.7 %copy-start.2 = (bf16[768,1024]{1,0:T(8,128)(2,1)S(1)}, bf16[768,1024]{1,0:T(8,128)(2,1)}, u32[]{:S(2)}) copy-start(bf16[768,1024]{1,0:T(8,128)(2,1)} %get-tuple-element.52.refs_0_) | copy-start | bytes 4718596
  284.6 31.3 %collective-permute-start.34 = (bf16[384,1024]{1,0:T(8,128)(2,1)}, bf16[384,1024]{1,0:T(8,128)(2,1)S(1)}, u32[]{:S(2)}, u32[]{:S(2)}) collective-permute-start(bf16[384,1024]{1,0:T(8,128)(2,1)} %get-tuple-element.67), channel_id=1, source_target_pairs={{0,2},{2,0},{4,6},{6,4},{1,3},{3,1},{5,7},{7,5},{8,10},{10,8},{12,... | collective-permute-start | bytes 2359304 | tf_op jit(solution)/shard_map/ppermute | solution.py:39
  285.1 30.8 %collective-permute-start.35 = (bf16[384,1024]{1,0:T(8,128)(2,1)}, bf16[384,1024]{1,0:T(8,128)(2,1)S(1)}, u32[]{:S(2)}, u32[]{:S(2)}) collective-permute-start(bf16[384,1024]{1,0:T(8,128)(2,1)} %get-tuple-element.68), channel_id=1, source_target_pairs={{0,4},{2,6},{4,0},{6,2},{1,5},{3,7},{5,1},{7,3},{8,12},{10,14},{12... | collective-permute-start | bytes 2359304 | tf_op jit(solution)/shard_map/ppermute | solution.py:39
  298.4 34.0 %collective-permute-start.33 = (bf16[384,1024]{1,0:T(8,128)(2,1)S(1)}, bf16[384,1024]{1,0:T(8,128)(2,1)S(1)}, u32[]{:S(2)}, u32[]{:S(2)}) collective-permute-start(bf16[384,1024]{1,0:T(8,128)(2,1)S(1)} %add.89), channel_id=1, source_target_pairs={{0,2},{2,0},{4,6},{6,4},{1,3},{3,1},{5,7},{7,5},{8,10},{10,8},{12,... | collective-permute-start | bytes 2359304 | tf_op jit(solution)/shard_map/ppermute | solution.py:39
  301.3 35.1 %copy-start.20 = (f32[1024]{0:T(1024)S(1)}, f32[1024]{0:T(1024)}, u32[]{:S(2)}) copy-start(f32[1024]{0:T(1024)} %param.35) | copy-start | bytes 12292
  301.3 31.0 %collective-permute-start.37 = (bf16[384,1024]{1,0:T(8,128)(2,1)S(1)}, bf16[384,1024]{1,0:T(8,128)(2,1)S(1)}, u32[]{:S(2)}, u32[]{:S(2)}) collective-permute-start(bf16[384,1024]{1,0:T(8,128)(2,1)S(1)} %add.91), channel_id=1, source_target_pairs={{0,4},{2,6},{4,0},{6,2},{1,5},{3,7},{5,1},{7,3},{8,12},{10,14},{12... | collective-permute-start | bytes 2359304 | tf_op jit(solution)/shard_map/ppermute | solution.py:39
  335.1 1.2 collective-permute-start.38
  (14 other events, 74.2 us)
Sparse Core Ops, SparseCore 0:
  25.7 88.2 all-gather.4
  144.5 83.6 all-gather.6
